TPU v7x, 32 devices: a whole 2x2x4 slice. The times are simulated.
32 devices in a mesh: fs: 8 (over z, y), tp: 4 (over x, core).
Axes of the slice: x: 2, y: 2, z: 4, core: 2. Of those that a mesh axis runs over, the one named last changes fastest.
Arguments:
- latent_in: bfloat16 [24576, 512], P('fs'), may hold values from -6 to 6
- query_cot: bfloat16 [24576, 1536], P('fs', 'tp'), may hold values from -6 to 6
- attn_out: bfloat16 [24576, 1024], P('fs'), may hold values from -6 to 6
- mix_cot: bfloat16 [24576, 2048], P('fs', 'tp'), may hold values from -6 to 6
- query_weight: float32 [512, 1536], P('fs', 'tp'), may hold values from -0.25 to 0.25
- output_weight: float32 [1024, 2048], P('fs', 'tp'), may hold values from -0.1875 to 0.1875
- query_factor: bfloat16 [512, 256], P('fs'), may hold values from -0.25 to 0.25
- output_factor: bfloat16 [1024, 256], P('fs'), may hold values from -0.1875 to 0.1875
- query_mean: float32 [256, 1536], P('fs', 'tp'), may hold values from -3 to 3
- query_square: float32 [256, 1536], P('fs', 'tp'), may hold values from 0.05 to 1
- output_mean: float32 [256, 2048], P('fs', 'tp'), may hold values from -3 to 3
- output_square: float32 [256, 2048], P('fs', 'tp'), may hold values from 0.05 to 1
Outputs:
- step_query: float32 [512, 1536], P('fs', 'tp')
- step_output: float32 [1024, 2048], P('fs', 'tp')
- new_query: float32 [512, 1536], P('fs', 'tp')
- new_output: float32 [1024, 2048], P('fs', 'tp')
- copy_query: bfloat16 [512, 1536], P(None, 'tp')
- copy_output: bfloat16 [1024, 2048], P(None, 'tp')
- query_mean_new: float32 [256, 1536], P('fs', 'tp')
- query_square_new: float32 [256, 1536], P('fs', 'tp')
- output_mean_new: float32 [256, 2048], P('fs', 'tp')
- output_square_new: float32 [256, 2048], P('fs', 'tp')
All inputs are finite; a program needn't handle non-finite values.
Results may differ from a plain program's by a relative error of at most 0.0085.
Values may be sent and summed in bfloat16 or wider, within the bound.
A program may use at most 64 MiB of HBM per device.

v0:
```python
import functools
import math

import jax
import jax.numpy as jnp
from jax import lax
from jax.experimental import pallas as pl
from jax.experimental.pallas import tpu as pltpu
from jax.sharding import PartitionSpec as P

MESH = pl.DeviceIdType.MESH
BF16 = jnp.bfloat16
F32 = jnp.float32
CHUNKS = 4


def grid_of(count):
    inner = max(d for d in range(1, count + 1) if count % d == 0 and d * d <= count)
    return count // inner, inner


def copies_of(nz, ny, nt):
    n = nz * ny
    per_gather = (nz - 1) + nz * (ny - 1)
    return per_gather + ny + 4 * per_gather + 2 * (nz + ny - 2) + (nt - 1) + (n - 1)


def over_rows(left, right):
    return lax.dot_general(left, right, (((0,), (0,)), ((), ())), preferred_element_type=F32)


def fused_kernel(
    nz, ny, nt, inv_root,
    latent_hbm, cot_hbm, attn_hbm, mix_hbm,
    wq_ref, wo_ref, fq_hbm, fo_hbm, qm_ref, qs_ref, om_ref, os_ref,
    fac, wq_all, wo_all, dq_all, do_all, low_q, low_o, total,
    latent, cot, attn, mix, grad_q, grad_o,
    part_q, part_o, yin_q, yin_o, acc_q, acc_o, zout_q, zout_o, zin_q, zin_o,
    tile_tp, tile_fs,
    load_sem, fac_sem, send_sem, recv_sem,
):
    n = nz * ny
    f = lax.axis_index("fs")
    t = lax.axis_index("tp")
    z, y = f // ny, f % ny
    half_cols = fac.shape[-1] // 2
    half = pl.ds(pl.multiple_of((t % 2) * half_cols, half_cols), half_cols)
    twin = t + 1 - 2 * (t % 2)
    rq = fq_hbm.shape[0]
    tokens = latent_hbm.shape[0]
    step = tokens // CHUNKS

    def load(k, pair, sem):
        rows = pl.ds(pl.multiple_of(k * step, step), step)
        return [
            pltpu.make_async_copy(src.at[rows, :], dst.at[rows, :], load_sem.at[k, sem + i])
            for i, (src, dst) in enumerate(pair)
        ]

    pair_o = ((attn_hbm, attn), (mix_hbm, mix))
    pair_q = ((latent_hbm, latent), (cot_hbm, cot))
    own = [
        pltpu.make_async_copy(fq_hbm.at[:, half], fac.at[z, y, pl.ds(0, rq), half], fac_sem.at[0]),
        pltpu.make_async_copy(
            fo_hbm.at[:, half], fac.at[z, y, pl.ds(rq, fo_hbm.shape[0]), half], fac_sem.at[1]
        ),
    ]
    for c in own:
        c.start()
    for k in range(CHUNKS):
        for c in load(k, pair_o, 0):
            c.start()
    for k in range(CHUNKS):
        for c in load(k, pair_q, 2):
            c.start()

    barrier = pltpu.get_barrier_semaphore()
    for d in range(1, n):
        pl.semaphore_signal(barrier, inc=1, device_id={"fs": (f + d) % n}, device_id_type=MESH)
    for d in range(1, nt):
        pl.semaphore_signal(barrier, inc=1, device_id={"tp": (t + d) % nt}, device_id_type=MESH)

    wq_all[z, y] = wq_ref[...].astype(BF16)
    wo_all[z, y] = wo_ref[...].astype(BF16)
    for c in own:
        c.wait()
    pl.semaphore_wait(barrier, n - 1 + nt - 1)

    started = []

    def send(src, dst, device):
        k = len(started)
        c = pltpu.make_async_remote_copy(
            src_ref=src, dst_ref=dst, send_sem=send_sem.at[k], recv_sem=recv_sem.at[k],
            device_id=device, device_id_type=MESH,
        )
        c.start()
        started.append(c)
        return c

    def to_z(d):
        return {"fs": ((z + d) % nz) * ny + y}

    def to_y(d):
        return {"fs": z * ny + (y + d) % ny}

    def z_send(block, ds):
        return {d: send(block(z), block(z), to_z(d)) for d in ds}

    def y_send(block, back):
        zz = (z + nz - back) % nz
        return [send(block(zz), block(zz), to_y(d)) for d in range(1, ny)]

    fac_block = lambda zz: fac.at[zz, y, :, half]
    wq_block = lambda zz: wq_all.at[zz, y]
    wo_block = lambda zz: wo_all.at[zz, y]
    dq_block = lambda zz: dq_all.at[zz, y]
    do_block = lambda zz: do_all.at[zz, y]

    far = range(1, nz)
    fac_z = z_send(fac_block, far)
    fac_y = y_send(fac_block, 0)
    early = far[: max(1, len(far) - 1)]
    w_z = {}
    for d in early:
        w_z[d] = (send(wo_block(z), wo_block(z), to_z(d)), send(wq_block(z), wq_block(z), to_z(d)))
    w_y = y_send(wo_block, 0) + y_send(wq_block, 0)

    grad_o[...] = jnp.zeros_like(grad_o)
    grad_q[...] = jnp.zeros_like(grad_q)

    def product(k, pair, sem, out):
        for c in load(k, pair, sem):
            c.wait()
        rows = pl.ds(pl.multiple_of(k * step, step), step)
        out[...] += over_rows(pair[1][1][rows, :], pair[0][1][rows, :])

    @pl.loop(0, CHUNKS // 2)
    def _(k):
        product(k, pair_o, 0, grad_o)

    for d in far:
        fac_z[d].wait_recv()
        fac_y += y_send(fac_block, d)
    swap = [send(fac.at[:, y, :, half], fac.at[:, y, :, half], {"tp": twin})]

    @pl.loop(CHUNKS // 2, CHUNKS)
    def _(k):
        product(k, pair_o, 0, grad_o)

    for c in fac_y:
        c.wait_recv()
    for d in range(1, ny):
        other = fac.at[:, (y + ny - d) % ny, :, half]
        swap.append(send(other, other, {"tp": twin}))

    @pl.loop(0, CHUNKS)
    def _(k):
        product(k, pair_q, 2, grad_q)

    for c in swap:
        c.wait_recv()

    rank = fac.shape[-1]
    block = rank // n

    def project(lo, hi, grad, part):
        factor = fac[:, :, lo:hi, :].reshape(n * (hi - lo), rank)
        g = grad[...]
        top = g.astype(BF16)
        rest = (g - top.astype(F32)).astype(BF16)
        dims = (((0,), (1,)), ((), ()))
        low = lax.dot_general(factor, top, dims, preferred_element_type=F32)
        low += lax.dot_general(factor, rest, dims, preferred_element_type=F32)
        low *= inv_root
        for i in range(nz):
            for j in range(ny):
                at = (i * ny + j) * block
                part[i, j] = low[at:at + block, :]

    matrices = (
        (rq, fac.shape[2], grad_o, part_o, yin_o, acc_o, zout_o, zin_o),
        (0, rq, grad_q, part_q, yin_q, acc_q, zout_q, zin_q),
    )
    y_in = []
    for lo, hi, grad, part, yin, acc, zout, zin in matrices:
        project(lo, hi, grad, part)
        copies = []
        for d in range(1, ny):
            yy = (y + d) % ny
            acc_send = yin.at[d - 1]
            for i in range(nz):
                yin[ny - 1 + d - 1, i] = part[i, yy].astype(BF16)
            copies.append(send(yin.at[ny - 1 + d - 1], acc_send, to_y(d)))
        y_in.append(copies)

    z_in = []
    for (lo, hi, grad, part, yin, acc, zout, zin), copies in zip(matrices, y_in):
        for i in range(nz):
            acc[i] = part[i, y]
        for d, c in enumerate(copies):
            c.wait_recv()
            for i in range(nz):
                acc[i] += yin[d, i].astype(F32)
        copies = []
        for d in far:
            zout[d - 1] = acc[(z + d) % nz].astype(BF16)
            copies.append(send(zout.at[d - 1], zin.at[d - 1], to_z(d)))
        z_in.append(copies)

    for d in far:
        if d not in w_z:
            w_z[d] = (send(wo_block(z), wo_block(z), to_z(d)), send(wq_block(z), wq_block(z), to_z(d)))

    def forward_weights(d):
        w_z[d][0].wait_recv()
        w_z[d][1].wait_recv()
        return y_send(wo_block, d) + y_send(wq_block, d)

    w_y += forward_weights(1) if nz > 1 else []

    sides = (
        (matrices[0], z_in[0], om_ref, os_ref, low_o, do_all, 1),
        (matrices[1], z_in[1], qm_ref, qs_ref, low_q, dq_all, 0),
    )
    d_z = []
    d_y = []
    for (_, _, _, _, _, acc, _, zin), copies, mean_ref, square_ref, low_ref, d_all, slot in sides:
        low = acc[z]
        for d, c in zip(far, copies):
            c.wait_recv()
            low += zin[d - 1].astype(F32)
        low_ref[...] = low
        mean_new = 0.8 * mean_ref[...] + 0.2 * low
        square_new = 0.9 * square_ref[...] + 0.1 * low * low
        direction = mean_new / jnp.sqrt(square_new)
        d_all[z, y] = direction.astype(BF16)
        tile_tp[0, slot] = jnp.broadcast_to(jnp.sum(direction * direction), tile_tp.shape[2:])
        where = lambda zz, d_all=d_all: d_all.at[zz, y]
        d_z.append((where, z_send(where, far)))
        d_y += y_send(where, 0)

    tiles = [
        send(tile_tp.at[0], tile_tp.at[d], {"tp": (t + d) % nt}) for d in range(1, nt)
    ]
    for c in tiles:
        c.wait_recv()
    tile_fs[0] = jnp.sum(tile_tp[...], axis=0)
    tiles = [
        send(tile_fs.at[0], tile_fs.at[d], {"fs": (f + d) % n}) for d in range(1, n)
    ]
    for d in far:
        for where, copies in d_z:
            copies[d].wait_recv()
            d_y += y_send(where, d)
    for d in far[1:]:
        w_y += forward_weights(d)
    for c in tiles:
        c.wait_recv()
    total[...] = jnp.sum(tile_fs[...], axis=0)
    for c in d_y + w_y:
        c.wait_recv()
    for c in started:
        c.wait_send()


def on_device(
    nz, ny, nt,
    latent_in, query_cot, attn_out, mix_cot, query_weight, output_weight,
    query_factor, output_factor, query_mean, query_square, output_mean, output_square,
):
    n = nz * ny
    tokens = latent_in.shape[0]
    inv_root = 1.0 / math.sqrt(tokens * n)
    rq, cq = query_weight.shape
    ro, co = output_weight.shape
    rank = query_factor.shape[1]
    block = rank // n
    vmem = pl.BlockSpec(memory_space=pltpu.VMEM)
    hbm = pl.BlockSpec(memory_space=pl.ANY)
    copies = copies_of(nz, ny, nt)
    fac, wq, wo, dq, do, low_q, low_o, total = pl.pallas_call(
        functools.partial(fused_kernel, nz, ny, nt, inv_root),
        name="moment_exchange",
        in_specs=[hbm] * 4 + [vmem] * 2 + [hbm] * 2 + [vmem] * 4,
        out_specs=[vmem] * 8,
        out_shape=[
            jax.ShapeDtypeStruct((nz, ny, rq + ro, rank), BF16),
            jax.ShapeDtypeStruct((nz, ny, rq, cq), BF16),
            jax.ShapeDtypeStruct((nz, ny, ro, co), BF16),
            jax.ShapeDtypeStruct((nz, ny, block, cq), BF16),
            jax.ShapeDtypeStruct((nz, ny, block, co), BF16),
            jax.ShapeDtypeStruct((block, cq), F32),
            jax.ShapeDtypeStruct((block, co), F32),
            jax.ShapeDtypeStruct((2, 8, 128), F32),
        ],
        scratch_shapes=[
            pltpu.VMEM(latent_in.shape, BF16),
            pltpu.VMEM(query_cot.shape, BF16),
            pltpu.VMEM(attn_out.shape, BF16),
            pltpu.VMEM(mix_cot.shape, BF16),
            pltpu.VMEM((cq, n * rq), F32),
            pltpu.VMEM((co, n * ro), F32),
            pltpu.VMEM((nz, ny, block, cq), F32),
            pltpu.VMEM((nz, ny, block, co), F32),
            pltpu.VMEM((2 * max(ny - 1, 1), nz, block, cq), BF16),
            pltpu.VMEM((2 * max(ny - 1, 1), nz, block, co), BF16),
            pltpu.VMEM((nz, block, cq), F32),
            pltpu.VMEM((nz, block, co), F32),
            pltpu.VMEM((max(nz - 1, 1), block, cq), BF16),
            pltpu.VMEM((max(nz - 1, 1), block, co), BF16),
            pltpu.VMEM((max(nz - 1, 1), block, cq), BF16),
            pltpu.VMEM((max(nz - 1, 1), block, co), BF16),
            pltpu.VMEM((nt, 2, 8, 128), F32),
            pltpu.VMEM((n, 2, 8, 128), F32),
            pltpu.SemaphoreType.DMA((CHUNKS, 4)),
            pltpu.SemaphoreType.DMA((2,)),
            pltpu.SemaphoreType.DMA((copies,)),
            pltpu.SemaphoreType.DMA((copies,)),
        ],
        compiler_params=pltpu.CompilerParams(
            collective_id=0, has_side_effects=True, vmem_limit_bytes=60 * 1024 * 1024
        ),
    )(
        latent_in, query_cot, attn_out, mix_cot, query_weight, output_weight,
        query_factor, output_factor, query_mean, query_square, output_mean, output_square,
    )

    def finish(factor, factor_all, direction, weight, weight_all, mean, square, low, slot):
        mean_new = 0.8 * mean + 0.2 * low
        square_new = 0.9 * square + 0.1 * low * low
        cols = weight.shape[1]
        scale = 1.0 / jnp.sqrt(total[slot, 0, 0] / (rank * cols * nt) + 0.25)
        direction = direction.reshape(rank, cols)
        step = jnp.dot(factor, direction, preferred_element_type=F32) * scale
        new = weight - 0.02 * step
        full = jnp.dot(factor_all.reshape(-1, rank), direction, preferred_element_type=F32) * scale
        copy = (weight_all.reshape(-1, cols).astype(F32) - 0.02 * full).astype(BF16)
        return step, new, copy, mean_new, square_new

    step_q, new_q, copy_q, mean_q, square_q = finish(
        query_factor, fac[:, :, :rq], dq, query_weight, wq, query_mean, query_square, low_q, 0
    )
    step_o, new_o, copy_o, mean_o, square_o = finish(
        output_factor, fac[:, :, rq:], do, output_weight, wo, output_mean, output_square, low_o, 1
    )
    return (step_q, step_o, new_q, new_o, copy_q, copy_o, mean_q, square_q, mean_o, square_o)


def solution(mesh):
    nz, ny = grid_of(mesh.shape["fs"])
    rows, both, cols = P("fs", None), P("fs", "tp"), P(None, "tp")
    return jax.shard_map(
        functools.partial(on_device, nz, ny, mesh.shape["tp"]),
        mesh=mesh,
        in_specs=(rows, both, rows, both, both, both, rows, rows, both, both, both, both),
        out_specs=(both, both, both, both, cols, cols, both, both, both, both),
        check_vma=False,
    )
```

profile of v0, /device:TPU:0, one launch (start us, length us, event | category | flops | bytes accessed | tf_op | source)
XLA Modules:
  0.0 71.6 jit_solution(4133091796622486584)
XLA Ops:
  0.6 0.0 copy-start.2
  0.7 0.0 copy-start
  0.7 0.0 copy-start.10
  0.7 0.0 copy-start.3
  0.7 59.4 %moment_exchange.1 = (bf16[4,2,192,256]{3,2,1,0:T(8,128)(2,1)}, bf16[4,2,64,384]{3,2,1,0:T(8,128)(2,1)}, bf16[4,2,128,512]{3,2,1,0:T(8,128)(2,1)}, bf16[4,2,32,3...) custom-call(bf16[3072,512]{1,0:T(8,128)(2,1)} %latent_hbm.1, ...), custom_call_target="tpu_custom_call" | custom-call | tf_op jit(solution)/shard_map/moment_exchange/pallas_call | solution.py:282
  60.1 0.0 copy-start.1
  60.1 0.0 copy-start.7
  60.1 0.0 copy-start.14
  60.1 1.3 %fusion.8 = (f32[1,1,1]{2,1,0:T(1,128)}, f32[1,1,1]{2,1,0:T(1,128)}) fusion(f32[2,8,128]{2,1,0:T(8,128)} %get-tuple-element.19), kind=kLoop, calls=%fused_computation.18 | loop fusion | bytes 16 | tf_op jit(solution)/shard_map/slice | solution.py:333
  62.1 0.0 copy-done.2
  62.1 0.0 copy-done.10
  62.1 1.8 %multiply_subtract_fusion.1 = (f32[64,384]{1,0:T(8,128)}, f32[64,384]{1,0:T(8,128)}) fusion(f32[64,384]{1,0:T(8,128)S(1)} %copy-done.2, f32[]{:T(128)} %bitcast.1, bf16[64,256]{1,0:T(8,128)(2,1)S(1)} %copy-done.10, bf16[256,384]{1,0:T(8,128)(2,1)} %bitcast.26), kind=kOutput, calls=%fused_computation.12 | convolution fusion | flops 12656640 | bytes 524292 | tf_op jit(solution)/shard_map/dot_general | solution.py:335
  63.9 0.0 copy-done
  63.9 0.1 copy.22
  64.7 0.0 copy-done.3
  64.7 1.2 %multiply_subtract_fusion = (f32[128,512]{0,1:T(8,128)S(1)}, f32[128,512]{0,1:T(8,128)S(1)}) fusion(f32[128,512]{0,1:T(8,128)S(1)} %copy.22, f32[]{:T(128)} %bitcast.4, bf16[256,512]{1,0:T(8,128)(2,1)} %bitcast.24, bf16[128,256]{1,0:T(8,128)(2,1)S(1)} %copy-done.3), kind=kOutput, calls=%fused_computation.10 | convolution fusion | flops 33751040 | bytes 1114116 | tf_op jit(solution)/shard_map/dot_general | solution.py:335
  65.9 0.0 copy-start.6
  66.0 0.0 copy-start.13
  66.0 0.8 %copy.23 = f32[128,512]{1,0:T(8,128)} copy(f32[128,512]{0,1:T(8,128)S(1)} %get-tuple-element.45) | data formatting | bytes 524288
  66.8 0.8 %copy.24 = f32[128,512]{1,0:T(8,128)} copy(f32[128,512]{0,1:T(8,128)S(1)} %get-tuple-element.44) | data formatting | bytes 524288
  67.6 0.0 copy-done.1
  67.7 0.0 copy-done.7
  67.7 0.0 copy-done.14
  67.7 1.0 %fusion.3 = bf16[512,384]{1,0:T(8,128)(2,1)} fusion(bf16[512,256]{1,0:T(8,128)(2,1)S(1)} %bitcast.23, bf16[256,384]{1,0:T(8,128)(2,1)S(1)} %bitcast.27, bf16[512,384]{1,0:T(8,128)(2,1)S(1)} %bitcast.29, f32[]{:T(128)} %bitcast.1), kind=kOutput, calls=%fused_computation.5 | convolution fusion | flops 101646336 | bytes 1245188 | tf_op jit(solution)/shard_map/dot_general | solution.py:337
  68.7 0.0 copy-start.8
  68.7 0.0 copy-start.9
  68.7 0.0 copy-start.12
  68.7 0.0 copy-start.4
  68.7 0.0 copy-start.5
  68.7 0.0 copy-start.11
  68.8 0.0 copy-done.6
  68.8 0.0 copy-done.13
  68.8 1.4 %fusion = bf16[1024,512]{1,0:T(8,128)(2,1)} fusion(bf16[1024,512]{1,0:T(8,128)(2,1)S(1)} %bitcast.28, bf16[1024,256]{1,0:T(8,128)(2,1)S(1)} %bitcast.22, bf16[256,512]{1,0:T(8,128)(2,1)S(1)} %bitcast.25, f32[]{:T(128)} %bitcast.4), kind=kOutput, calls=%fused_computation.1 | convolution fusion | flops 271056896 | bytes 2883588 | tf_op jit(solution)/shard_map/dot_general | solution.py:337
  70.3 0.0 copy-done.8
  70.3 0.0 copy-done.9
  70.3 0.0 copy-done.12
  70.3 0.7 fusion.7
  70.9 0.0 copy-done.4
  70.9 0.0 copy-done.5
  70.9 0.0 copy-done.11
  70.9 0.7 fusion.6
  (2 shorter events, 0.1 us)
Async XLA Ops:
  0.6 61.4 %copy-start.2 = (f32[64,384]{1,0:T(8,128)S(1)}, f32[64,384]{1,0:T(8,128)}, u32[]{:S(2)}) copy-start(f32[64,384]{1,0:T(8,128)} %wq_ref.1) | copy-start | bytes 294916
  0.7 63.2 %copy-start = (f32[128,512]{1,0:T(8,128)S(1)}, f32[128,512]{1,0:T(8,128)}, u32[]{:S(2)}) copy-start(f32[128,512]{1,0:T(8,128)} %wo_ref.1) | copy-start | bytes 786436
  0.7 61.4 %copy-start.10 = (bf16[64,256]{1,0:T(8,128)(2,1)S(1)}, bf16[64,256]{1,0:T(8,128)(2,1)}, u32[]{:S(2)}) copy-start(bf16[64,256]{1,0:T(8,128)(2,1)} %fq_hbm.1) | copy-start | bytes 98308
  0.7 64.0 %copy-start.3 = (bf16[128,256]{1,0:T(8,128)(2,1)S(1)}, bf16[128,256]{1,0:T(8,128)(2,1)}, u32[]{:S(2)}) copy-start(bf16[128,256]{1,0:T(8,128)(2,1)} %fo_hbm.1) | copy-start | bytes 196612
  60.1 7.6 %copy-start.1 = (bf16[4,2,192,256]{3,2,1,0:T(8,128)(2,1)S(1)}, bf16[4,2,192,256]{3,2,1,0:T(8,128)(2,1)}, u32[]{:S(2)}) copy-start(bf16[4,2,192,256]{3,2,1,0:T(8,128)(2,1)} %get-tuple-element.22) | copy-start | bytes 2359300
  60.1 7.6 %copy-start.7 = (bf16[4,2,32,384]{3,2,1,0:T(8,128)(2,1)S(1)}, bf16[4,2,32,384]{3,2,1,0:T(8,128)(2,1)}, u32[]{:S(2)}) copy-start(bf16[4,2,32,384]{3,2,1,0:T(8,128)(2,1)} %get-tuple-element.18) | copy-start | bytes 589828
  60.1 7.6 %copy-start.14 = (bf16[4,2,64,384]{3,2,1,0:T(8,128)(2,1)S(1)}, bf16[4,2,64,384]{3,2,1,0:T(8,128)(2,1)}, u32[]{:S(2)}) copy-start(bf16[4,2,64,384]{3,2,1,0:T(8,128)(2,1)} %get-tuple-element.21) | copy-start | bytes 1179652
  65.9 2.9 %copy-start.6 = (bf16[4,2,32,512]{3,2,1,0:T(8,128)(2,1)S(1)}, bf16[4,2,32,512]{3,2,1,0:T(8,128)(2,1)}, u32[]{:S(2)}) copy-start(bf16[4,2,32,512]{3,2,1,0:T(8,128)(2,1)} %get-tuple-element.20) | copy-start | bytes 786436
  66.0 2.9 %copy-start.13 = (bf16[4,2,128,512]{3,2,1,0:T(8,128)(2,1)S(1)}, bf16[4,2,128,512]{3,2,1,0:T(8,128)(2,1)}, u32[]{:S(2)}) copy-start(bf16[4,2,128,512]{3,2,1,0:T(8,128)(2,1)} %get-tuple-element.23) | copy-start | bytes 3145732
  68.7 1.5 %copy-start.8 = (f32[32,384]{1,0:T(8,128)S(1)}, f32[32,384]{1,0:T(8,128)}, u32[]{:S(2)}) copy-start(f32[32,384]{1,0:T(8,128)} %qm_ref.1) | copy-start | bytes 147460
  68.7 1.5 %copy-start.9 = (f32[32,384]{1,0:T(8,128)S(1)}, f32[32,384]{1,0:T(8,128)}, u32[]{:S(2)}) copy-start(f32[32,384]{1,0:T(8,128)} %qs_ref.1) | copy-start | bytes 147460
  68.7 1.5 %copy-start.12 = (f32[32,384]{1,0:T(8,128)S(1)}, f32[32,384]{1,0:T(8,128)}, u32[]{:S(2)}) copy-start(f32[32,384]{1,0:T(8,128)} %get-tuple-element.24) | copy-start | bytes 147460
  68.7 2.2 %copy-start.4 = (f32[32,512]{1,0:T(8,128)S(1)}, f32[32,512]{1,0:T(8,128)}, u32[]{:S(2)}) copy-start(f32[32,512]{1,0:T(8,128)} %om_ref.1) | copy-start | bytes 196612
  68.7 2.2 %copy-start.5 = (f32[32,512]{1,0:T(8,128)S(1)}, f32[32,512]{1,0:T(8,128)}, u32[]{:S(2)}) copy-start(f32[32,512]{1,0:T(8,128)} %os_ref.1) | copy-start | bytes 196612
  68.7 2.2 %copy-start.11 = (f32[32,512]{1,0:T(8,128)S(1)}, f32[32,512]{1,0:T(8,128)}, u32[]{:S(2)}) copy-start(f32[32,512]{1,0:T(8,128)} %get-tuple-element.25) | copy-start | bytes 196612
where the time goes:
time: 71.8 us; the launch traced here: 71.6 us
  Pallas kernels  59.4 us (83%)
  matrix products  5.47 us (8%)
  local copies, waits for them, and re-layouts  3.22 us (4%)
  between operations  2.23 us (3%)
  other arithmetic  1.33 us (2%)
    pallas_call x1, Pallas kernels, on_device(): pl.pallas_call(functools.partial(fused_kernel, nz, ny, nt, inv_root), nam...  59.4 us
    dot_general x2, matrix products, finish(): step = jnp.dot(factor, direction, preferred_element_type=F32) * scale  2.99 us
    dot_general x2, matrix products, finish(): jnp.dot(factor_all.reshape(-1, rank), direction, preferred_element_type=F32)  2.49 us
    unnamed x33, local copies, waits for them, and re-layouts  1.86 us

commit v1 on v0

v1 whole, which is shorter than its diff:
```python
import functools
import math

import jax
import jax.numpy as jnp
from jax import lax
from jax.experimental import pallas as pl
from jax.experimental.pallas import tpu as pltpu
from jax.sharding import PartitionSpec as P

MESH = pl.DeviceIdType.MESH
BF16 = jnp.bfloat16
F32 = jnp.float32
CHUNKS = 4


def grid_of(count):
    inner = max(d for d in range(1, count + 1) if count % d == 0 and d * d <= count)
    return count // inner, inner


def semaphores_of(nz, ny, nt):
    z_kinds, y_kinds = 2 + 2 + 2 + 2, 2 + 2 + 2
    return z_kinds * nz + y_kinds * nz * (ny - 1) + 2 * (ny - 1) + 4 * ny + nt + nz * ny + 4


def over_rows(left, right):
    return lax.dot_general(left, right, (((0,), (0,)), ((), ())), preferred_element_type=F32)


def exchange_kernel(
    nz, ny, nt, inv_root,
    latent_hbm, cot_hbm, attn_hbm, mix_hbm, wq_hbm, wo_hbm, fq_hbm, fo_hbm,
    qm_hbm, qs_hbm, om_hbm, os_hbm,
    fq_all, fo_all, wq_all, wo_all, dq_all, do_all, total, qm_new, qs_new, om_new, os_new,
    latent, cot, attn, mix, wq, wo, qm, qs, om, os_, grad_q, grad_o,
    part_q, part_o, yin_q, yin_o, acc_q, acc_o, zout_q, zout_o, zin_q, zin_o,
    tile_tp, tile_fs,
    load_sem, own_sem, send_sem, recv_sem,
):
    n = nz * ny
    f = lax.axis_index("fs")
    t = lax.axis_index("tp")
    z, y = f // ny, f % ny
    half_cols = fq_all.shape[-1] // 2
    half = pl.ds(pl.multiple_of((t % 2) * half_cols, half_cols), half_cols)
    twin = t + 1 - 2 * (t % 2)
    step = latent_hbm.shape[0] // CHUNKS

    barrier = pltpu.get_barrier_semaphore()
    for d in range(1, n):
        pl.semaphore_signal(barrier, inc=1, device_id={"fs": (f + d) % n}, device_id_type=MESH)
    for d in range(1, nt):
        pl.semaphore_signal(barrier, inc=1, device_id={"tp": (t + d) % nt}, device_id_type=MESH)

    own = [
        pltpu.make_async_copy(src, dst, own_sem.at[i])
        for i, (src, dst) in enumerate((
            (fo_hbm.at[:, half], fo_all.at[z, y, :, half]),
            (fq_hbm.at[:, half], fq_all.at[z, y, :, half]),
            (wo_hbm, wo), (wq_hbm, wq),
            (om_hbm, om), (os_hbm, os_), (qm_hbm, qm), (qs_hbm, qs),
        ))
    ]
    for c in own[:4]:
        c.start()

    def load(k, pair, sem):
        rows = pl.ds(pl.multiple_of(k * step, step), step)
        return [
            pltpu.make_async_copy(src.at[rows, :], dst.at[rows, :], load_sem.at[k, sem + i])
            for i, (src, dst) in enumerate(pair)
        ]

    pair_o = ((attn_hbm, attn), (mix_hbm, mix))
    pair_q = ((latent_hbm, latent), (cot_hbm, cot))
    with jax.named_scope("own"):
        for c in own[:4]:
            c.wait()
    for k in range(CHUNKS):
        for c in load(k, pair_o, 0):
            c.start()
    for k in range(CHUNKS):
        for c in load(k, pair_q, 2):
            c.start()
    for c in own[4:]:
        c.start()
    wo_all[z, y] = wo[...].astype(BF16)
    wq_all[z, y] = wq[...].astype(BF16)
    with jax.named_scope("barrier"):
        pl.semaphore_wait(barrier, n - 1 + nt - 1)

    used = [0]
    sent = []

    def room(count):
        at = used[0]
        used[0] = at + count
        return at

    def remote(src, dst, device, at, to):
        return pltpu.make_async_remote_copy(
            src_ref=src, dst_ref=dst, send_sem=send_sem.at[at], recv_sem=recv_sem.at[to],
            device_id=device, device_id_type=MESH,
        )

    def launch(c):
        c.start()
        sent.append(c)
        return c

    lower, upper = z, nz - 1 - z
    both = jnp.minimum(lower, upper)

    def near(k):
        paired = k < 2 * both
        away = jnp.where(paired, k // 2 + 1, k - both + 1)
        down = jnp.where(paired, k % 2 == 0, lower > upper)
        return jnp.where(down, z - away, z + away)

    others = [near(k) for k in range(nz - 1)]

    class Along:
        def __init__(self, block, landing=None):
            self.block, self.landing, self.at = block, landing or block, room(nz)

        def to(self, zz):
            return remote(
                self.block(z) if self.landing is self.block else self.block(zz), self.landing(z),
                {"fs": zz * ny + y}, self.at + zz, self.at + z,
            )

        def wait(self, zz):
            remote(
                self.landing(zz), self.landing(zz), {"fs": zz * ny + y}, self.at + zz, self.at + zz
            ).wait_recv()

    class Across:
        def __init__(self, block):
            self.block, self.at = block, room(nz * (ny - 1))

        def send(self, zz):
            for d in range(1, ny):
                k = self.at + (d - 1) * nz + zz
                launch(remote(
                    self.block(zz, y), self.block(zz, y), {"fs": z * ny + (y + d) % ny}, k, k
                ))

        def wait(self, zz):
            for d in range(1, ny):
                k = self.at + (d - 1) * nz + zz
                block = self.block(zz, (y + ny - d) % ny)
                remote(block, block, {"fs": z * ny + (y + d) % ny}, k, k).wait_recv()

    fo_z = Along(lambda zz: fo_all.at[zz, y, :, half])
    fq_z = Along(lambda zz: fq_all.at[zz, y, :, half])
    fo_y = Across(lambda zz, yy: fo_all.at[zz, yy, :, half])
    fq_y = Across(lambda zz, yy: fq_all.at[zz, yy, :, half])
    wo_z = Along(lambda zz: wo_all.at[zz, y])
    wq_z = Along(lambda zz: wq_all.at[zz, y])
    wo_y = Across(lambda zz, yy: wo_all.at[zz, yy])
    wq_y = Across(lambda zz, yy: wq_all.at[zz, yy])
    do_z = Along(lambda zz: do_all.at[zz, y])
    dq_z = Along(lambda zz: dq_all.at[zz, y])
    do_y = Across(lambda zz, yy: do_all.at[zz, yy])
    dq_y = Across(lambda zz, yy: dq_all.at[zz, yy])

    for fac_z, fac_y in ((fo_z, fo_y), (fq_z, fq_y)):
        for zz in others:
            launch(fac_z.to(zz))
        fac_y.send(z)

    through = nz >= 3
    inside = jnp.logical_and(z > 0, z < nz - 1)
    far = []
    for k, zz in enumerate(others):
        for w_z in (wq_z, wo_z):
            c = w_z.to(zz)
            if through and k == nz - 2:
                far.append(c)
                pl.when(inside)(c.start)
            else:
                launch(c)
    wo_y.send(z)

    def product(k, pair, sem, out):
        for c in load(k, pair, sem):
            c.wait()
        rows = pl.ds(pl.multiple_of(k * step, step), step)
        new = over_rows(pair[1][1][rows, :], pair[0][1][rows, :])
        out[...] += new

    def products(lo, hi, pair, sem, out):
        @pl.loop(lo, hi)
        def _(k):
            product(k, pair, sem, out)

    grad_o[...] = jnp.zeros_like(grad_o)
    grad_q[...] = jnp.zeros_like(grad_q)
    swaps = {}

    def swap(all_, yy):
        block = all_.at[:, yy, :, half]
        k = room(1)
        return launch(remote(block, block, {"tp": twin}, k, k))

    with jax.named_scope("prod_o"):
        products(0, CHUNKS - 1, pair_o, 0, grad_o)
    for zz in others:
        with jax.named_scope("wait_foz"):
            fo_z.wait(zz)
        fo_y.send(zz)
    swaps["o"] = [swap(fo_all, y)]
    with jax.named_scope("prod_o"):
        products(CHUNKS - 1, CHUNKS, pair_o, 0, grad_o)
    for zz in others:
        with jax.named_scope("wait_fqz"):
            fq_z.wait(zz)
        fq_y.send(zz)
    swaps["q"] = [swap(fq_all, y)]
    wq_y.send(z)
    with jax.named_scope("prod_q"):
        products(0, CHUNKS, pair_q, 2, grad_q)

    rank = fq_all.shape[-1]
    block = rank // n

    def project(factor_all, grad, part):
        factor = factor_all[...].reshape(-1, rank)
        low = lax.dot_general(
            factor, grad[...].astype(BF16), (((0,), (1,)), ((), ())), preferred_element_type=F32
        ) * inv_root
        for i in range(nz):
            for j in range(ny):
                at = (i * ny + j) * block
                part[i, j] = low[at:at + block, :]

    matrices = (
        ("o", fo_all, fo_y, grad_o, part_o, yin_o, acc_o, zout_o, zin_o),
        ("q", fq_all, fq_y, grad_q, part_q, yin_q, acc_q, zout_q, zin_q),
    )
    y_in = []
    for name, all_, fac_y, grad, part, yin, acc, zout, zin in matrices:
        with jax.named_scope("wait_fy"):
            for zz in [z] + others:
                fac_y.wait(zz)
        for d in range(1, ny):
            swaps[name].append(swap(all_, (y + ny - d) % ny))
        with jax.named_scope("wait_swap"):
            for c in swaps[name]:
                c.wait_recv()
        with jax.named_scope("project"):
            project(all_, grad, part)
        copies = []
        for d in range(1, ny):
            yy = (y + d) % ny
            for i in range(nz):
                yin[ny - 1 + d - 1, i] = part[i, yy].astype(BF16)
            k = room(1)
            copies.append(launch(remote(
                yin.at[ny - 1 + d - 1], yin.at[d - 1], {"fs": z * ny + yy}, k, k
            )))
        y_in.append(copies)

    def forward_weights(k):
        zz = others[k]
        with jax.named_scope("wait_wz"):
            wq_z.wait(zz)
            wo_z.wait(zz)
        wo_y.send(zz)
        wq_y.send(zz)

    if nz > 1:
        forward_weights(0)

    low_z = []
    for (name, _, _, _, part, yin, acc, zout, zin), copies in zip(matrices, y_in):
        for i in range(nz):
            acc[i] = part[i, y]
        for d, c in enumerate(copies):
            with jax.named_scope("wait_y"):
                c.wait_recv()
            for i in range(nz):
                acc[i] += yin[d, i].astype(F32)
        along = Along(lambda zz, zout=zout: zout.at[zz], lambda zz, zin=zin: zin.at[zz])
        for zz in others:
            zout[zz] = acc[zz].astype(BF16)
            launch(along.to(zz))
        low_z.append(along)

    if nz > 2:
        forward_weights(1)

    if through:
        ahead = []
        for edge, here in ((0, nz - 2), (nz - 1, 1)):
            for w_z in (wq_z, wo_z):
                k = room(1)
                ahead.append((here, edge, w_z, remote(
                    w_z.block(edge), w_z.block(edge), {"fs": (nz - 1 - edge) * ny + y},
                    k, w_z.at + edge,
                )))

    sides = (
        (matrices[0], low_z[0], om, os_, om_new, os_new, do_all, do_z, do_y, 1),
        (matrices[1], low_z[1], qm, qs, qm_new, qs_new, dq_all, dq_z, dq_y, 0),
    )
    for c in own[4:]:
        c.wait()
    for (_, _, _, _, _, _, acc, _, zin), along, mean, square, mean_out, square_out, d_all, d_z, d_y, slot in sides:
        low = acc[z]
        for zz in others:
            with jax.named_scope("wait_z"):
                along.wait(zz)
            low += zin[zz].astype(F32)
        mean_new = 0.8 * mean[...] + 0.2 * low
        square_new = 0.9 * square[...] + 0.1 * low * low
        mean_out[...] = mean_new
        square_out[...] = square_new
        direction = mean_new / jnp.sqrt(square_new)
        d_all[z, y] = direction.astype(BF16)
        for zz in others:
            launch(d_z.to(zz))
        d_y.send(z)
        tile_tp[0, slot] = jnp.broadcast_to(jnp.sum(direction * direction), tile_tp.shape[2:])

    tiles = []
    for d in range(1, nt):
        k = room(1)
        tiles.append(launch(remote(tile_tp.at[0], tile_tp.at[d], {"tp": (t + d) % nt}, k, k)))

    if through:
        @pl.when(inside)
        def _():
            with jax.named_scope("wait_far"):
                wq_z.wait(others[nz - 2])
                wo_z.wait(others[nz - 2])
        for here, edge, w_z, c in ahead:
            pl.when(z == here)(c.start)

    with jax.named_scope("wait_tp"):
        for c in tiles:
            c.wait_recv()
    tile_fs[0] = jnp.sum(tile_tp[...], axis=0)
    tiles = []
    for d in range(1, n):
        k = room(1)
        tiles.append(launch(remote(tile_fs.at[0], tile_fs.at[d], {"fs": (f + d) % n}, k, k)))
    for d_z, d_y in ((do_z, do_y), (dq_z, dq_y)):
        for zz in others:
            with jax.named_scope("wait_dz"):
                d_z.wait(zz)
            d_y.send(zz)

    for k in range(2, nz - 1):
        zz = others[k]
        if through and k == nz - 2:
            with jax.named_scope("wait_wz_last"):
                @pl.when(jnp.logical_not(inside))
                def _():
                    wq_z.wait(zz)
                    wo_z.wait(zz)
        else:
            wq_z.wait(zz)
            wo_z.wait(zz)
        wo_y.send(zz)
        wq_y.send(zz)

    with jax.named_scope("wait_fs"):
        for c in tiles:
            c.wait_recv()
    total[...] = jnp.sum(tile_fs[...], axis=0)
    with jax.named_scope("wait_dy"):
        for zz in [z] + others:
            do_y.wait(zz)
            dq_y.wait(zz)
    with jax.named_scope("wait_wy"):
        for zz in [z] + others:
            wo_y.wait(zz)
            wq_y.wait(zz)
    for c in sent:
        c.wait_send()
    for c in far:
        pl.when(inside)(c.wait_send)
    if through:
        for here, edge, w_z, c in ahead:
            pl.when(z == here)(c.wait_send)


def finish_kernel(
    nz, ny, nt,
    fq_all, fo_all, wq_all, wo_all, dq_all, do_all, total, wq, wo, qm, qs, om, os_,
    step_q_hbm, step_o_hbm, new_q_hbm, new_o_hbm, copy_q_hbm, copy_o_hbm,
    qm_hbm, qs_hbm, om_hbm, os_hbm,
    step_q, step_o, new_q, new_o, copy_q, copy_o,
    sem,
):
    f = lax.axis_index("fs")
    z, y = f // ny, f % ny
    started = []

    def put(src, dst):
        c = pltpu.make_async_copy(src, dst, sem.at[len(started)])
        c.start()
        started.append(c)

    for src, dst in ((qm, qm_hbm), (qs, qs_hbm), (om, om_hbm), (os_, os_hbm)):
        put(src, dst)
    rank = fq_all.shape[-1]
    for slot, f_all, w_all, d_all, w, step, new, copy, step_hbm, new_hbm, copy_hbm in (
        (1, fo_all, wo_all, do_all, wo, step_o, new_o, copy_o, step_o_hbm, new_o_hbm, copy_o_hbm),
        (0, fq_all, wq_all, dq_all, wq, step_q, new_q, copy_q, step_q_hbm, new_q_hbm, copy_q_hbm),
    ):
        cols = w.shape[1]
        scale = lax.rsqrt(total[slot] / (rank * cols * nt) + 0.25)[0:1, 0:1]
        direction = d_all[...].reshape(rank, cols)
        rows = f_all.shape[2]
        for i in range(nz):
            full = jnp.dot(
                f_all[i].reshape(ny * rows, rank), direction, preferred_element_type=F32
            ) * scale
            at = pl.ds(i * ny * rows, ny * rows)
            old = w_all[i].reshape(ny * rows, cols).astype(F32)
            copy[at, :] = (old - 0.02 * full).astype(BF16)
            put(copy.at[at, :], copy_hbm.at[at, :])
        own = jnp.dot(f_all[z, y], direction, preferred_element_type=F32) * scale
        step[...] = own
        new[...] = w[...] - 0.02 * own
        put(step, step_hbm)
        put(new, new_hbm)
    for c in started:
        c.wait()


def on_device(
    nz, ny, nt,
    latent_in, query_cot, attn_out, mix_cot, query_weight, output_weight,
    query_factor, output_factor, query_mean, query_square, output_mean, output_square,
):
    n = nz * ny
    tokens = latent_in.shape[0]
    inv_root = 1.0 / math.sqrt(tokens * n)
    rq, cq = query_weight.shape
    ro, co = output_weight.shape
    rank = query_factor.shape[1]
    block = rank // n
    vmem = pl.BlockSpec(memory_space=pltpu.VMEM)
    hbm = pl.BlockSpec(memory_space=pltpu.HBM)
    copies = semaphores_of(nz, ny, nt)
    fq, fo, wq, wo, dq, do, total, qm, qs, om, os_ = pl.pallas_call(
        functools.partial(exchange_kernel, nz, ny, nt, inv_root),
        name="moment_exchange",
        in_specs=[hbm] * 12,
        out_specs=[vmem] * 11,
        out_shape=[
            jax.ShapeDtypeStruct((nz, ny, rq, rank), BF16),
            jax.ShapeDtypeStruct((nz, ny, ro, rank), BF16),
            jax.ShapeDtypeStruct((nz, ny, rq, cq), BF16),
            jax.ShapeDtypeStruct((nz, ny, ro, co), BF16),
            jax.ShapeDtypeStruct((nz, ny, block, cq), BF16),
            jax.ShapeDtypeStruct((nz, ny, block, co), BF16),
            jax.ShapeDtypeStruct((2, 8, 128), F32),
            jax.ShapeDtypeStruct((block, cq), F32),
            jax.ShapeDtypeStruct((block, cq), F32),
            jax.ShapeDtypeStruct((block, co), F32),
            jax.ShapeDtypeStruct((block, co), F32),
        ],
        scratch_shapes=[
            pltpu.VMEM(latent_in.shape, BF16),
            pltpu.VMEM(query_cot.shape, BF16),
            pltpu.VMEM(attn_out.shape, BF16),
            pltpu.VMEM(mix_cot.shape, BF16),
            pltpu.VMEM((rq, cq), F32),
            pltpu.VMEM((ro, co), F32),
            pltpu.VMEM((block, cq), F32),
            pltpu.VMEM((block, cq), F32),
            pltpu.VMEM((block, co), F32),
            pltpu.VMEM((block, co), F32),
            pltpu.VMEM((cq, n * rq), F32),
            pltpu.VMEM((co, n * ro), F32),
            pltpu.VMEM((nz, ny, block, cq), F32),
            pltpu.VMEM((nz, ny, block, co), F32),
            pltpu.VMEM((2 * max(ny - 1, 1), nz, block, cq), BF16),
            pltpu.VMEM((2 * max(ny - 1, 1), nz, block, co), BF16),
            pltpu.VMEM((nz, block, cq), F32),
            pltpu.VMEM((nz, block, co), F32),
            pltpu.VMEM((nz, block, cq), BF16),
            pltpu.VMEM((nz, block, co), BF16),
            pltpu.VMEM((nz, block, cq), BF16),
            pltpu.VMEM((nz, block, co), BF16),
            pltpu.VMEM((nt, 2, 8, 128), F32),
            pltpu.VMEM((n, 2, 8, 128), F32),
            pltpu.SemaphoreType.DMA((CHUNKS, 4)),
            pltpu.SemaphoreType.DMA((8,)),
            pltpu.SemaphoreType.DMA((copies,)),
            pltpu.SemaphoreType.DMA((copies,)),
        ],
        compiler_params=pltpu.CompilerParams(
            collective_id=0, has_side_effects=True, vmem_limit_bytes=40 * 1024 * 1024
        ),
    )(*(pltpu.with_memory_space_constraint(a, pltpu.HBM) for a in (
        latent_in, query_cot, attn_out, mix_cot, query_weight, output_weight,
        query_factor, output_factor, query_mean, query_square, output_mean, output_square,
    )))
    shapes = (
        ((rq, cq), F32), ((ro, co), F32), ((rq, cq), F32), ((ro, co), F32),
        ((n * rq, cq), BF16), ((n * ro, co), BF16),
        ((block, cq), F32), ((block, cq), F32), ((block, co), F32), ((block, co), F32),
    )
    return pl.pallas_call(
        functools.partial(finish_kernel, nz, ny, nt),
        name="finish",
        in_specs=[vmem] * 13,
        out_specs=[hbm] * 10,
        out_shape=[jax.ShapeDtypeStruct(*s) for s in shapes],
        scratch_shapes=[pltpu.VMEM(*s) for s in shapes[:6]]
        + [pltpu.SemaphoreType.DMA((2 * nz + 8,))],
        compiler_params=pltpu.CompilerParams(vmem_limit_bytes=20 * 1024 * 1024),
    )(fq, fo, wq, wo, dq, do, total, query_weight, output_weight, qm, qs, om, os_)


def solution(mesh):
    nz, ny = grid_of(mesh.shape["fs"])
    rows, both, cols = P("fs", None), P("fs", "tp"), P(None, "tp")
    return jax.shard_map(
        functools.partial(on_device, nz, ny, mesh.shape["tp"]),
        mesh=mesh,
        in_specs=(rows, both, rows, both, both, both, rows, rows, both, both, both, both),
        out_specs=(both, both, both, both, cols, cols, both, both, both, both),
        check_vma=False,
    )
```

time: 71.8 us -> 45.8 us (0.64)
  Pallas kernels: 59.4 us -> 45 us
  matrix products: 5.47 us -> 0 us
  local copies, waits for them, and re-layouts: 3.22 us -> 0.01 us
  between operations: 2.23 us -> 0.69 us
  other arithmetic: 1.33 us -> 0 us
    pallas_call x1 -> x2, Pallas kernels: 59.4 us -> 45 us  [the longest x1 43.2 us: on_device(): pl.pallas_call(functools.partial(exchange_kernel, nz, ny, nt, inv_root),...]
    dot_general x4 -> x0, matrix products: 5.47 us -> none  [the longest x2 2.99 us: finish(): step = jnp.dot(factor, direction, preferred_element_type=F32) * scale]
    unnamed x33 -> x4, local copies, waits for them, and re-layouts: 1.86 us -> 0.01 us
    slice x3 -> x0, local copies, waits for them, and re-layouts: 1.36 us -> none  [the longest x1 1.31 us: finish(): scale = 1.0 / jnp.sqrt(total[slot, 0, 0] / (rank * cols * nt) + 0.25)]
    add x2 -> x0, other arithmetic: 1.33 us -> none  [finish(): square_new = 0.9 * square + 0.1 * low * low]
where the time goes in v1:
time: 45.8 us; the launch traced here: 45.7 us
  Pallas kernels  45 us (98%)
  between operations  0.69 us (2%)
    pallas_call x1, Pallas kernels, on_device(): pl.pallas_call(functools.partial(exchange_kernel, nz, ny, nt, inv_root),...  43.2 us
    pallas_call x1, Pallas kernels, on_device(): pl.pallas_call(functools.partial(finish_kernel, nz, ny, nt), name='finish...  1.72 us

profile of v1, /device:TPU:0, one launch (start us, length us, event | category | flops | bytes accessed | tf_op | source)
XLA Modules:
  0.0 45.7 jit_solution(8184237684462846743)
XLA Ops:
  0.6 0.0 copy-start
  0.7 0.0 copy-start.1
  0.7 43.2 %moment_exchange.1 = (bf16[4,2,64,256]{3,2,1,0:T(8,128)(2,1)S(1)}, bf16[4,2,128,256]{3,2,1,0:T(8,128)(2,1)S(1)}, bf16[4,2,64,384]{3,2,1,0:T(8,128)(2,1)S(1)}, bf...) custom-call(bf16[3072,512]{1,0:T(8,128)(2,1)} %latent_hbm.1, ...), custom_call_target="tpu_custom_call" | custom-call | tf_op jit(solution)/shard_map/moment_exchange/pallas_call | solution.py:450
  43.9 0.0 copy-done
  43.9 0.0 copy-done.1
  43.9 1.7 %finish.1 = (f32[64,384]{1,0:T(8,128)}, f32[128,512]{1,0:T(8,128)}, f32[64,384]{1,0:T(8,128)}, f32[128,512]{1,0:T(8,128)}, bf16[512,384]{1,0:T(8,128)(2,1)}, /*i...) custom-call(bf16[4,2,64,256]{3,2,1,0:T(8,128)(2,1)S(1)} %get-tuple-e, ...), custom_call_target="tpu_custom_call" | custom-call | tf_op jit(solution)/shard_map/finish/pallas_call | solution.py:510
Async XLA Ops:
  0.6 43.3 %copy-start = (f32[128,512]{1,0:T(8,128)S(1)}, f32[128,512]{1,0:T(8,128)}, u32[]{:S(2)}) copy-start(f32[128,512]{1,0:T(8,128)} %wo.1) | copy-start | bytes 786436
  0.7 43.3 %copy-start.1 = (f32[64,384]{1,0:T(8,128)S(1)}, f32[64,384]{1,0:T(8,128)}, u32[]{:S(2)}) copy-start(f32[64,384]{1,0:T(8,128)} %wq.1) | copy-start | bytes 294916

commit v2 on v1

--- a/solution.py
+++ b/solution.py
@@ -21,7 +21,7 @@
 
 def semaphores_of(nz, ny, nt):
     z_kinds, y_kinds = 2 + 2 + 2 + 2, 2 + 2 + 2
-    return z_kinds * nz + y_kinds * nz * (ny - 1) + 2 * (ny - 1) + 4 * ny + nt + nz * ny + 4
+    return z_kinds * nz + y_kinds * nz * (ny - 1) + 6 * (ny - 1) + 2 * ny + nt + nz * ny + 4
 
 
 def over_rows(left, right):
@@ -35,15 +35,16 @@
     fq_all, fo_all, wq_all, wo_all, dq_all, do_all, total, qm_new, qs_new, om_new, os_new,
     latent, cot, attn, mix, wq, wo, qm, qs, om, os_, grad_q, grad_o,
     part_q, part_o, yin_q, yin_o, acc_q, acc_o, zout_q, zout_o, zin_q, zin_o,
-    tile_tp, tile_fs,
+    tile_tp, tile_fs, rounded_q, rounded_o,
     load_sem, own_sem, send_sem, recv_sem,
 ):
     n = nz * ny
     f = lax.axis_index("fs")
     t = lax.axis_index("tp")
     z, y = f // ny, f % ny
-    half_cols = fq_all.shape[-1] // 2
-    half = pl.ds(pl.multiple_of((t % 2) * half_cols, half_cols), half_cols)
+    half_cols = fq_all.shape[-1]
+    core = t % 2
+    half = pl.ds(pl.multiple_of(core * half_cols, half_cols), half_cols)
     twin = t + 1 - 2 * (t % 2)
     step = latent_hbm.shape[0] // CHUNKS
 
@@ -56,8 +57,8 @@
     own = [
         pltpu.make_async_copy(src, dst, own_sem.at[i])
         for i, (src, dst) in enumerate((
-            (fo_hbm.at[:, half], fo_all.at[z, y, :, half]),
-            (fq_hbm.at[:, half], fq_all.at[z, y, :, half]),
+            (fo_hbm.at[:, half], fo_all.at[core, z, y]),
+            (fq_hbm.at[:, half], fq_all.at[core, z, y]),
             (wo_hbm, wo), (wq_hbm, wq),
             (om_hbm, om), (os_hbm, os_), (qm_hbm, qm), (qs_hbm, qs),
         ))
@@ -115,7 +116,7 @@
     def near(k):
         paired = k < 2 * both
         away = jnp.where(paired, k // 2 + 1, k - both + 1)
-        down = jnp.where(paired, k % 2 == 0, lower > upper)
+        down = jnp.where(paired, (k + z) % 2 == 1, lower > upper)
         return jnp.where(down, z - away, z + away)
 
     others = [near(k) for k in range(nz - 1)]
@@ -139,12 +140,16 @@
         def __init__(self, block):
             self.block, self.at = block, room(nz * (ny - 1))
 
+        def copies(self, zz):
+            ks = [self.at + (d - 1) * nz + zz for d in range(1, ny)]
+            return [
+                remote(self.block(zz, y), self.block(zz, y), {"fs": z * ny + (y + d) % ny}, k, k)
+                for d, k in zip(range(1, ny), ks)
+            ]
+
         def send(self, zz):
-            for d in range(1, ny):
-                k = self.at + (d - 1) * nz + zz
-                launch(remote(
-                    self.block(zz, y), self.block(zz, y), {"fs": z * ny + (y + d) % ny}, k, k
-                ))
+            for c in self.copies(zz):
+                launch(c)
 
         def wait(self, zz):
             for d in range(1, ny):
@@ -152,10 +157,10 @@
                 block = self.block(zz, (y + ny - d) % ny)
                 remote(block, block, {"fs": z * ny + (y + d) % ny}, k, k).wait_recv()
 
-    fo_z = Along(lambda zz: fo_all.at[zz, y, :, half])
-    fq_z = Along(lambda zz: fq_all.at[zz, y, :, half])
-    fo_y = Across(lambda zz, yy: fo_all.at[zz, yy, :, half])
-    fq_y = Across(lambda zz, yy: fq_all.at[zz, yy, :, half])
+    fo_z = Along(lambda zz: fo_all.at[core, zz, y])
+    fq_z = Along(lambda zz: fq_all.at[core, zz, y])
+    fo_y = Across(lambda zz, yy: fo_all.at[core, zz, yy])
+    fq_y = Across(lambda zz, yy: fq_all.at[core, zz, yy])
     wo_z = Along(lambda zz: wo_all.at[zz, y])
     wq_z = Along(lambda zz: wq_all.at[zz, y])
     wo_y = Across(lambda zz, yy: wo_all.at[zz, yy])
@@ -169,19 +174,23 @@
         for zz in others:
             launch(fac_z.to(zz))
         fac_y.send(z)
+    wo_y.send(z)
 
     through = nz >= 3
+    mated = nz % 2 == 0
     inside = jnp.logical_and(z > 0, z < nz - 1)
     far = []
-    for k, zz in enumerate(others):
-        for w_z in (wq_z, wo_z):
-            c = w_z.to(zz)
+
+    def send_weights(w_z, ks):
+        for k in ks:
+            c = w_z.to(others[k])
             if through and k == nz - 2:
                 far.append(c)
                 pl.when(inside)(c.start)
             else:
                 launch(c)
-    wo_y.send(z)
+
+    outward = list(reversed(range(nz - 1)))
 
     def product(k, pair, sem, out):
         for c in load(k, pair, sem):
@@ -200,19 +209,28 @@
     swaps = {}
 
     def swap(all_, yy):
-        block = all_.at[:, yy, :, half]
+        block = all_.at[core, :, yy]
         k = room(1)
         return launch(remote(block, block, {"tp": twin}, k, k))
 
+    early = CHUNKS // 2
     with jax.named_scope("prod_o"):
-        products(0, CHUNKS - 1, pair_o, 0, grad_o)
-    for zz in others:
+        products(0, early, pair_o, 0, grad_o)
+    for k, zz in enumerate(others):
         with jax.named_scope("wait_foz"):
             fo_z.wait(zz)
         fo_y.send(zz)
+        if k == min(1, nz - 2):
+            send_weights(wo_z, outward)
+            send_weights(wq_z, [0])
+        if early < CHUNKS:
+            with jax.named_scope("prod_o"):
+                products(early, early + 1, pair_o, 0, grad_o)
+            early += 1
     swaps["o"] = [swap(fo_all, y)]
     with jax.named_scope("prod_o"):
-        products(CHUNKS - 1, CHUNKS, pair_o, 0, grad_o)
+        if early < CHUNKS:
+            products(early, CHUNKS, pair_o, 0, grad_o)
     for zz in others:
         with jax.named_scope("wait_fqz"):
             fq_z.wait(zz)
@@ -222,92 +240,139 @@
     with jax.named_scope("prod_q"):
         products(0, CHUNKS, pair_q, 2, grad_q)
 
-    rank = fq_all.shape[-1]
+    rank = 2 * half_cols
     block = rank // n
-
-    def project(factor_all, grad, part):
-        factor = factor_all[...].reshape(-1, rank)
+    per_half = nz // 2
+
+    def project(h, factor_all, grad, part):
+        factor = factor_all[h].reshape(-1, half_cols)
         low = lax.dot_general(
-            factor, grad[...].astype(BF16), (((0,), (1,)), ((), ())), preferred_element_type=F32
+            factor, grad[...], (((0,), (1,)), ((), ())), preferred_element_type=F32
         ) * inv_root
-        for i in range(nz):
+        for i in range(per_half):
             for j in range(ny):
                 at = (i * ny + j) * block
-                part[i, j] = low[at:at + block, :]
+                part[h * per_half + i, j] = low[at:at + block, :]
 
     matrices = (
-        ("o", fo_all, fo_y, grad_o, part_o, yin_o, acc_o, zout_o, zin_o),
-        ("q", fq_all, fq_y, grad_q, part_q, yin_q, acc_q, zout_q, zin_q),
+        ("o", fo_all, fo_y, grad_o, rounded_o, part_o, yin_o, acc_o, zout_o, zin_o),
+        ("q", fq_all, fq_y, grad_q, rounded_q, part_q, yin_q, acc_q, zout_q, zin_q),
     )
-    y_in = []
-    for name, all_, fac_y, grad, part, yin, acc, zout, zin in matrices:
+    units = []
+    for name, all_, fac_y, grad, rounded, part, yin, acc, zout, zin in matrices:
+        rounded[...] = grad[...].astype(BF16)
+        along = Along(lambda zz, zout=zout: zout.at[zz], lambda zz, zin=zin: zin.at[zz])
         with jax.named_scope("wait_fy"):
             for zz in [z] + others:
                 fac_y.wait(zz)
         for d in range(1, ny):
             swaps[name].append(swap(all_, (y + ny - d) % ny))
-        with jax.named_scope("wait_swap"):
-            for c in swaps[name]:
-                c.wait_recv()
-        with jax.named_scope("project"):
-            project(all_, grad, part)
-        copies = []
+        for turn, h in enumerate((core, 1 - core)):
+            if turn:
+                with jax.named_scope("wait_swap"):
+                    for c in swaps[name]:
+                        c.wait_recv()
+            with jax.named_scope("project"):
+                project(h, all_, rounded, part)
+            rows = pl.ds(h * per_half, per_half)
+            copies = []
+            for d in range(1, ny):
+                yy = (y + d) % ny
+                for i in range(per_half):
+                    yin[ny - 1 + d - 1, h * per_half + i] = part[h * per_half + i, yy].astype(BF16)
+                k = room(1)
+                copies.append(launch(remote(
+                    yin.at[ny - 1 + d - 1, rows], yin.at[d - 1, rows], {"fs": z * ny + yy}, k, k
+                )))
+            units.append((h, part, yin, acc, zout, along, copies))
+
+    def forward(k, w_z, w_y):
+        with jax.named_scope("wait_wz"):
+            w_z.wait(others[k])
+        w_y.send(others[k])
+
+    if nz > 1 and not mated:
+        forward(0, wo_z, wo_y)
+        forward(0, wq_z, wq_y)
+
+    ahead = []
+
+    def relay(w_z):
+        if not through:
+            return
+        mine = []
+        for edge, here in ((0, nz - 2), (nz - 1, 1)):
+            k = room(1)
+            mine.append((here, remote(
+                w_z.block(edge), w_z.block(edge), {"fs": (nz - 1 - edge) * ny + y},
+                k, w_z.at + edge,
+            )))
+
+        @pl.when(inside)
+        def _():
+            with jax.named_scope("wait_far"):
+                w_z.wait(others[nz - 2])
+        for here, c in mine:
+            pl.when(z == here)(c.start)
+        ahead.extend(mine)
+
+    def forward_far(w_z, w_y, at_edge):
+        if not through:
+            return
+        if at_edge:
+            @pl.when(jnp.logical_not(inside))
+            def _():
+                with jax.named_scope("wait_wz_last"):
+                    w_z.wait(others[nz - 2])
+        cs = w_y.copies(others[nz - 2])
+        for c in cs:
+            pl.when(jnp.logical_not(inside) if at_edge else inside)(c.start)
+        fars.append((at_edge, cs))
+
+    fars = []
+
+    def hand_over(w_y):
+        mate = z + 1 - 2 * (z % 2)
+        out = []
         for d in range(1, ny):
             yy = (y + d) % ny
-            for i in range(nz):
-                yin[ny - 1 + d - 1, i] = part[i, yy].astype(BF16)
             k = room(1)
-            copies.append(launch(remote(
-                yin.at[ny - 1 + d - 1], yin.at[d - 1], {"fs": z * ny + yy}, k, k
-            )))
-        y_in.append(copies)
-
-    def forward_weights(k):
-        zz = others[k]
-        with jax.named_scope("wait_wz"):
-            wq_z.wait(zz)
-            wo_z.wait(zz)
-        wo_y.send(zz)
-        wq_y.send(zz)
-
-    if nz > 1:
-        forward_weights(0)
-
-    low_z = []
-    for (name, _, _, _, part, yin, acc, zout, zin), copies in zip(matrices, y_in):
-        for i in range(nz):
-            acc[i] = part[i, y]
+            out.append(remote(w_y.block(z, yy), w_y.block(z, yy), {"fs": mate * ny + y}, k, k))
+            out[-1].got = remote(
+                w_y.block(mate, yy), w_y.block(mate, yy), {"fs": mate * ny + y}, k, k
+            )
+        return out
+
+    low_sent = []
+    for turn, (h, part, yin, acc, zout, along, copies) in enumerate(units):
+        if turn == 1 and nz > 3:
+            forward(1, wo_z, wo_y)
+        if turn == 2:
+            relay(wo_z)
+        for i in range(per_half):
+            acc[h * per_half + i] = part[h * per_half + i, y]
         for d, c in enumerate(copies):
             with jax.named_scope("wait_y"):
                 c.wait_recv()
-            for i in range(nz):
-                acc[i] += yin[d, i].astype(F32)
-        along = Along(lambda zz, zout=zout: zout.at[zz], lambda zz, zin=zin: zin.at[zz])
-        for zz in others:
+            for i in range(per_half):
+                acc[h * per_half + i] += yin[d, h * per_half + i].astype(F32)
+        for i in range(per_half):
+            zz = h * per_half + i
             zout[zz] = acc[zz].astype(BF16)
-            launch(along.to(zz))
-        low_z.append(along)
-
-    if nz > 2:
-        forward_weights(1)
-
-    if through:
-        ahead = []
-        for edge, here in ((0, nz - 2), (nz - 1, 1)):
-            for w_z in (wq_z, wo_z):
-                k = room(1)
-                ahead.append((here, edge, w_z, remote(
-                    w_z.block(edge), w_z.block(edge), {"fs": (nz - 1 - edge) * ny + y},
-                    k, w_z.at + edge,
-                )))
+            c = along.to(zz)
+            pl.when(zz != z)(c.start)
+            low_sent.append((zz, c))
 
     sides = (
-        (matrices[0], low_z[0], om, os_, om_new, os_new, do_all, do_z, do_y, 1),
-        (matrices[1], low_z[1], qm, qs, qm_new, qs_new, dq_all, dq_z, dq_y, 0),
+        (matrices[0], units[0][5], om, os_, om_new, os_new, do_all, do_z, do_y),
+        (matrices[1], units[2][5], qm, qs, qm_new, qs_new, dq_all, dq_z, dq_y),
     )
+    forward_far(wo_z, wo_y, False)
     for c in own[4:]:
         c.wait()
-    for (_, _, _, _, _, _, acc, _, zin), along, mean, square, mean_out, square_out, d_all, d_z, d_y, slot in sides:
+    squares = []
+    for matrix, along, mean, square, mean_out, square_out, d_all, d_z, d_y in sides:
+        acc, zin = matrix[7], matrix[9]
         low = acc[z]
         for zz in others:
             with jax.named_scope("wait_z"):
@@ -322,22 +387,26 @@
         for zz in others:
             launch(d_z.to(zz))
         d_y.send(z)
-        tile_tp[0, slot] = jnp.broadcast_to(jnp.sum(direction * direction), tile_tp.shape[2:])
+        squares.append(jnp.sum(direction * direction))
+    lanes = lax.broadcasted_iota(jnp.int32, tile_tp.shape[1:], 1)
+    tile_tp[0] = jnp.where(lanes < tile_tp.shape[2] // 2, squares[1], squares[0])
 
     tiles = []
     for d in range(1, nt):
         k = room(1)
         tiles.append(launch(remote(tile_tp.at[0], tile_tp.at[d], {"tp": (t + d) % nt}, k, k)))
 
-    if through:
-        @pl.when(inside)
-        def _():
-            with jax.named_scope("wait_far"):
-                wq_z.wait(others[nz - 2])
-                wo_z.wait(others[nz - 2])
-        for here, edge, w_z, c in ahead:
-            pl.when(z == here)(c.start)
-
+    forward_far(wo_z, wo_y, True)
+
+    def forward_directions(d_z, d_y):
+        for zz in others:
+            with jax.named_scope("wait_dz"):
+                d_z.wait(zz)
+            d_y.send(zz)
+
+    forward_directions(do_z, do_y)
+    late = [k for k in outward if k not in [0]]
+    send_weights(wq_z, late)
     with jax.named_scope("wait_tp"):
         for c in tiles:
             c.wait_recv()
@@ -346,25 +415,20 @@
     for d in range(1, n):
         k = room(1)
         tiles.append(launch(remote(tile_fs.at[0], tile_fs.at[d], {"fs": (f + d) % n}, k, k)))
-    for d_z, d_y in ((do_z, do_y), (dq_z, dq_y)):
-        for zz in others:
-            with jax.named_scope("wait_dz"):
-                d_z.wait(zz)
-            d_y.send(zz)
-
-    for k in range(2, nz - 1):
-        zz = others[k]
-        if through and k == nz - 2:
-            with jax.named_scope("wait_wz_last"):
-                @pl.when(jnp.logical_not(inside))
-                def _():
-                    wq_z.wait(zz)
-                    wo_z.wait(zz)
-        else:
-            wq_z.wait(zz)
-            wo_z.wait(zz)
-        wo_y.send(zz)
-        wq_y.send(zz)
+    forward_directions(dq_z, dq_y)
+    relay(wq_z)
+    handed = []
+    if mated:
+        for w_y in (wo_y, wq_y):
+            w_y.wait(z)
+            for c in hand_over(w_y):
+                handed.append(launch(c))
+    for k in range(2, nz - 2):
+        forward(k, wo_z, wo_y)
+    for k in range(1, nz - 2):
+        forward(k, wq_z, wq_y)
+    forward_far(wq_z, wq_y, False)
+    forward_far(wq_z, wq_y, True)
 
     with jax.named_scope("wait_fs"):
         for c in tiles:
@@ -375,16 +439,26 @@
             do_y.wait(zz)
             dq_y.wait(zz)
     with jax.named_scope("wait_wy"):
-        for zz in [z] + others:
+        for c in handed:
+            c.got.wait_recv()
+        if mated:
+            wo_z.wait(others[0])
+            wq_z.wait(others[0])
+        for zz in others[1:] if mated else [z] + others:
             wo_y.wait(zz)
             wq_y.wait(zz)
-    for c in sent:
-        c.wait_send()
+    with jax.named_scope("wait_send"):
+        for c in sent:
+            c.wait_send()
+    for zz, c in low_sent:
+        pl.when(zz != z)(c.wait_send)
     for c in far:
         pl.when(inside)(c.wait_send)
-    if through:
-        for here, edge, w_z, c in ahead:
-            pl.when(z == here)(c.wait_send)
+    for here, c in ahead:
+        pl.when(z == here)(c.wait_send)
+    for at_edge, cs in fars:
+        for c in cs:
+            pl.when(jnp.logical_not(inside) if at_edge else inside)(c.wait_send)
 
 
 def finish_kernel(
@@ -406,24 +480,30 @@
 
     for src, dst in ((qm, qm_hbm), (qs, qs_hbm), (om, om_hbm), (os_, os_hbm)):
         put(src, dst)
-    rank = fq_all.shape[-1]
+    rank = 2 * fq_all.shape[-1]
+    middle = total.shape[1] // 2
     for slot, f_all, w_all, d_all, w, step, new, copy, step_hbm, new_hbm, copy_hbm in (
-        (1, fo_all, wo_all, do_all, wo, step_o, new_o, copy_o, step_o_hbm, new_o_hbm, copy_o_hbm),
+        (middle, fo_all, wo_all, do_all, wo, step_o, new_o, copy_o, step_o_hbm, new_o_hbm, copy_o_hbm),
         (0, fq_all, wq_all, dq_all, wq, step_q, new_q, copy_q, step_q_hbm, new_q_hbm, copy_q_hbm),
     ):
         cols = w.shape[1]
-        scale = lax.rsqrt(total[slot] / (rank * cols * nt) + 0.25)[0:1, 0:1]
+        scale = lax.rsqrt(total[...] / (rank * cols * nt) + 0.25)[:, slot:slot + 1]
         direction = d_all[...].reshape(rank, cols)
-        rows = f_all.shape[2]
+        rows = f_all.shape[3]
+
+        def factor_rows(i, f_all=f_all):
+            return jnp.concatenate([f_all[h, i].reshape(-1, rank // 2) for h in range(2)], axis=1)
+
         for i in range(nz):
             full = jnp.dot(
-                f_all[i].reshape(ny * rows, rank), direction, preferred_element_type=F32
+                factor_rows(i), direction, preferred_element_type=F32
             ) * scale
             at = pl.ds(i * ny * rows, ny * rows)
             old = w_all[i].reshape(ny * rows, cols).astype(F32)
             copy[at, :] = (old - 0.02 * full).astype(BF16)
             put(copy.at[at, :], copy_hbm.at[at, :])
-        own = jnp.dot(f_all[z, y], direction, preferred_element_type=F32) * scale
+        mine = jnp.concatenate([f_all[h, z, y] for h in range(2)], axis=1)
+        own = jnp.dot(mine, direction, preferred_element_type=F32) * scale
         step[...] = own
         new[...] = w[...] - 0.02 * own
         put(step, step_hbm)
@@ -447,19 +527,29 @@
     vmem = pl.BlockSpec(memory_space=pltpu.VMEM)
     hbm = pl.BlockSpec(memory_space=pltpu.HBM)
     copies = semaphores_of(nz, ny, nt)
+
+    def exchange(*refs):
+        pl.run_scoped(
+            functools.partial(exchange_kernel, nz, ny, nt, inv_root, *refs),
+            pltpu.SemaphoreType.DMA((CHUNKS, 4)),
+            pltpu.SemaphoreType.DMA((8,)),
+            pltpu.SemaphoreType.DMA((copies,)),
+            pltpu.SemaphoreType.DMA((copies,)),
+        )
+
     fq, fo, wq, wo, dq, do, total, qm, qs, om, os_ = pl.pallas_call(
-        functools.partial(exchange_kernel, nz, ny, nt, inv_root),
+        exchange,
         name="moment_exchange",
         in_specs=[hbm] * 12,
         out_specs=[vmem] * 11,
         out_shape=[
-            jax.ShapeDtypeStruct((nz, ny, rq, rank), BF16),
-            jax.ShapeDtypeStruct((nz, ny, ro, rank), BF16),
+            jax.ShapeDtypeStruct((2, nz, ny, rq, rank // 2), BF16),
+            jax.ShapeDtypeStruct((2, nz, ny, ro, rank // 2), BF16),
             jax.ShapeDtypeStruct((nz, ny, rq, cq), BF16),
             jax.ShapeDtypeStruct((nz, ny, ro, co), BF16),
             jax.ShapeDtypeStruct((nz, ny, block, cq), BF16),
             jax.ShapeDtypeStruct((nz, ny, block, co), BF16),
-            jax.ShapeDtypeStruct((2, 8, 128), F32),
+            jax.ShapeDtypeStruct((1, 128), F32),
             jax.ShapeDtypeStruct((block, cq), F32),
             jax.ShapeDtypeStruct((block, cq), F32),
             jax.ShapeDtypeStruct((block, co), F32),
@@ -488,12 +578,10 @@
             pltpu.VMEM((nz, block, co), BF16),
             pltpu.VMEM((nz, block, cq), BF16),
             pltpu.VMEM((nz, block, co), BF16),
-            pltpu.VMEM((nt, 2, 8, 128), F32),
-            pltpu.VMEM((n, 2, 8, 128), F32),
-            pltpu.SemaphoreType.DMA((CHUNKS, 4)),
-            pltpu.SemaphoreType.DMA((8,)),
-            pltpu.SemaphoreType.DMA((copies,)),
-            pltpu.SemaphoreType.DMA((copies,)),
+            pltpu.VMEM((nt, 1, 128), F32),
+            pltpu.VMEM((n, 1, 128), F32),
+            pltpu.VMEM((cq, n * rq), BF16),
+            pltpu.VMEM((co, n * ro), BF16),
         ],
         compiler_params=pltpu.CompilerParams(
             collective_id=0, has_side_effects=True, vmem_limit_bytes=40 * 1024 * 1024
@@ -507,14 +595,20 @@
         ((n * rq, cq), BF16), ((n * ro, co), BF16),
         ((block, cq), F32), ((block, cq), F32), ((block, co), F32), ((block, co), F32),
     )
+
+    def finish(*refs):
+        pl.run_scoped(
+            functools.partial(finish_kernel, nz, ny, nt, *refs),
+            pltpu.SemaphoreType.DMA((2 * nz + 8,)),
+        )
+
     return pl.pallas_call(
-        functools.partial(finish_kernel, nz, ny, nt),
+        finish,
         name="finish",
         in_specs=[vmem] * 13,
         out_specs=[hbm] * 10,
         out_shape=[jax.ShapeDtypeStruct(*s) for s in shapes],
-        scratch_shapes=[pltpu.VMEM(*s) for s in shapes[:6]]
-        + [pltpu.SemaphoreType.DMA((2 * nz + 8,))],
+        scratch_shapes=[pltpu.VMEM(*s) for s in shapes[:6]],
         compiler_params=pltpu.CompilerParams(vmem_limit_bytes=20 * 1024 * 1024),
     )(fq, fo, wq, wo, dq, do, total, query_weight, output_weight, qm, qs, om, os_)
 

time: 45.8 us -> 42.8 us (0.934)
  Pallas kernels: 45 us -> 42 us
    pallas_call x2, Pallas kernels: 45 us -> 42 us  [the longest x1 40.4 us: on_device(): pl.pallas_call(exchange, name='moment_exchange', in_specs=[hbm] * 12, out...]
where the time goes in v2:
time: 42.8 us; the launch traced here: 42.7 us
  Pallas kernels  42 us (98%)
  between operations  0.69 us (2%)
    pallas_call x1, Pallas kernels, on_device(): pl.pallas_call(exchange, name='moment_exchange', in_specs=[hbm] * 12, out...  40.4 us
    pallas_call x1, Pallas kernels, on_device(): pl.pallas_call(finish, name='finish', in_specs=[vmem] * 13, out_specs=[hb...  1.58 us

profile of v2, /device:TPU:0, one launch (start us, length us, event | category | flops | bytes accessed | tf_op | source)
XLA Modules:
  0.0 42.7 jit_solution(16438175072842604009)
XLA Ops:
  0.6 0.0 copy-start
  0.7 0.0 copy-start.1
  0.7 40.4 %moment_exchange.1 = (bf16[2,4,2,64,128]{4,3,2,1,0:T(8,128)(2,1)S(1)}, bf16[2,4,2,128,128]{4,3,2,1,0:T(8,128)(2,1)S(1)}, bf16[4,2,64,384]{3,2,1,0:T(8,128)(2,1)S...) custom-call(bf16[3072,512]{1,0:T(8,128)(2,1)} %refs_0_.1, ...), custom_call_target="tpu_custom_call" | custom-call | tf_op jit(solution)/shard_map/moment_exchange/pallas_call | solution.py:540
  41.1 0.0 copy-done
  41.1 0.0 copy-done.1
  41.1 1.6 %finish.1 = (f32[64,384]{1,0:T(8,128)}, f32[128,512]{1,0:T(8,128)}, f32[64,384]{1,0:T(8,128)}, f32[128,512]{1,0:T(8,128)}, bf16[512,384]{1,0:T(8,128)(2,1)}, /*i...) custom-call(bf16[2,4,2,64,128]{4,3,2,1,0:T(8,128)(2,1)S(1)} %get-tup, ...), custom_call_target="tpu_custom_call" | custom-call | tf_op jit(solution)/shard_map/finish/pallas_call | solution.py:605
Async XLA Ops:
  0.6 40.4 %copy-start = (f32[128,512]{1,0:T(8,128)S(1)}, f32[128,512]{1,0:T(8,128)}, u32[]{:S(2)}) copy-start(f32[128,512]{1,0:T(8,128)} %refs_8_.3) | copy-start | bytes 786436
  0.7 40.4 %copy-start.1 = (f32[64,384]{1,0:T(8,128)S(1)}, f32[64,384]{1,0:T(8,128)}, u32[]{:S(2)}) copy-start(f32[64,384]{1,0:T(8,128)} %refs_7_.3) | copy-start | bytes 294916

commit v3 on v2

--- a/solution.py
+++ b/solution.py
@@ -79,10 +79,10 @@
         for c in own[:4]:
             c.wait()
     for k in range(CHUNKS):
-        for c in load(k, pair_o, 0):
+        for c in load(k, pair_q, 2):
             c.start()
     for k in range(CHUNKS):
-        for c in load(k, pair_q, 2):
+        for c in load(k, pair_o, 0):
             c.start()
     for c in own[4:]:
         c.start()
@@ -170,7 +170,7 @@
     do_y = Across(lambda zz, yy: do_all.at[zz, yy])
     dq_y = Across(lambda zz, yy: dq_all.at[zz, yy])
 
-    for fac_z, fac_y in ((fo_z, fo_y), (fq_z, fq_y)):
+    for fac_z, fac_y in ((fq_z, fq_y), (fo_z, fo_y)):
         for zz in others:
             launch(fac_z.to(zz))
         fac_y.send(z)
@@ -181,10 +181,10 @@
     inside = jnp.logical_and(z > 0, z < nz - 1)
     far = []
 
-    def send_weights(w_z, ks):
+    def send_weights(w_z, ks, relayed=False):
         for k in ks:
             c = w_z.to(others[k])
-            if through and k == nz - 2:
+            if relayed and through and k == nz - 2:
                 far.append(c)
                 pl.when(inside)(c.start)
             else:
@@ -213,32 +213,32 @@
         k = room(1)
         return launch(remote(block, block, {"tp": twin}, k, k))
 
-    early = CHUNKS // 2
-    with jax.named_scope("prod_o"):
-        products(0, early, pair_o, 0, grad_o)
-    for k, zz in enumerate(others):
-        with jax.named_scope("wait_foz"):
-            fo_z.wait(zz)
-        fo_y.send(zz)
-        if k == min(1, nz - 2):
-            send_weights(wo_z, outward)
-            send_weights(wq_z, [0])
-        if early < CHUNKS:
+    done = 0
+
+    def more_o(upto):
+        nonlocal done
+        if done < upto:
             with jax.named_scope("prod_o"):
-                products(early, early + 1, pair_o, 0, grad_o)
-            early += 1
-    swaps["o"] = [swap(fo_all, y)]
-    with jax.named_scope("prod_o"):
-        if early < CHUNKS:
-            products(early, CHUNKS, pair_o, 0, grad_o)
+                products(done, upto, pair_o, 0, grad_o)
+            done = upto
+
+    with jax.named_scope("prod_q"):
+        products(0, CHUNKS, pair_q, 2, grad_q)
+    more_o(1)
     for zz in others:
         with jax.named_scope("wait_fqz"):
             fq_z.wait(zz)
         fq_y.send(zz)
     swaps["q"] = [swap(fq_all, y)]
-    wq_y.send(z)
-    with jax.named_scope("prod_q"):
-        products(0, CHUNKS, pair_q, 2, grad_q)
+    send_weights(wo_z, outward, True)
+    for k, zz in enumerate(others):
+        if k == 0:
+            more_o(2)
+        with jax.named_scope("wait_foz"):
+            fo_z.wait(zz)
+        fo_y.send(zz)
+    swaps["o"] = [swap(fo_all, y)]
+    more_o(CHUNKS - 1)
 
     rank = 2 * half_cols
     block = rank // n
@@ -255,11 +255,14 @@
                 part[h * per_half + i, j] = low[at:at + block, :]
 
     matrices = (
+        ("q", fq_all, fq_y, grad_q, rounded_q, part_q, yin_q, acc_q, zout_q, zin_q),
         ("o", fo_all, fo_y, grad_o, rounded_o, part_o, yin_o, acc_o, zout_o, zin_o),
-        ("q", fq_all, fq_y, grad_q, rounded_q, part_q, yin_q, acc_q, zout_q, zin_q),
     )
     units = []
     for name, all_, fac_y, grad, rounded, part, yin, acc, zout, zin in matrices:
+        if name == "o":
+            wq_y.send(z)
+            more_o(CHUNKS)
         rounded[...] = grad[...].astype(BF16)
         along = Along(lambda zz, zout=zout: zout.at[zz], lambda zz, zin=zin: zin.at[zz])
         with jax.named_scope("wait_fy"):
@@ -345,10 +348,10 @@
 
     low_sent = []
     for turn, (h, part, yin, acc, zout, along, copies) in enumerate(units):
-        if turn == 1 and nz > 3:
-            forward(1, wo_z, wo_y)
         if turn == 2:
             relay(wo_z)
+        if turn == 3 and nz > 3:
+            forward(1, wo_z, wo_y)
         for i in range(per_half):
             acc[h * per_half + i] = part[h * per_half + i, y]
         for d, c in enumerate(copies):
@@ -364,8 +367,8 @@
             low_sent.append((zz, c))
 
     sides = (
-        (matrices[0], units[0][5], om, os_, om_new, os_new, do_all, do_z, do_y),
-        (matrices[1], units[2][5], qm, qs, qm_new, qs_new, dq_all, dq_z, dq_y),
+        (matrices[0], units[0][5], qm, qs, qm_new, qs_new, dq_all, dq_z, dq_y),
+        (matrices[1], units[2][5], om, os_, om_new, os_new, do_all, do_z, do_y),
     )
     forward_far(wo_z, wo_y, False)
     for c in own[4:]:
@@ -388,15 +391,16 @@
             launch(d_z.to(zz))
         d_y.send(z)
         squares.append(jnp.sum(direction * direction))
+        if len(squares) == 1:
+            forward_far(wo_z, wo_y, True)
     lanes = lax.broadcasted_iota(jnp.int32, tile_tp.shape[1:], 1)
-    tile_tp[0] = jnp.where(lanes < tile_tp.shape[2] // 2, squares[1], squares[0])
+    tile_tp[0] = jnp.where(lanes < tile_tp.shape[2] // 2, squares[0], squares[1])
 
     tiles = []
     for d in range(1, nt):
         k = room(1)
         tiles.append(launch(remote(tile_tp.at[0], tile_tp.at[d], {"tp": (t + d) % nt}, k, k)))
-
-    forward_far(wo_z, wo_y, True)
+    send_weights(wq_z, outward)
 
     def forward_directions(d_z, d_y):
         for zz in others:
@@ -404,9 +408,16 @@
                 d_z.wait(zz)
             d_y.send(zz)
 
-    forward_directions(do_z, do_y)
-    late = [k for k in outward if k not in [0]]
-    send_weights(wq_z, late)
+    handed = []
+
+    def hand(w_y):
+        if mated:
+            w_y.wait(z)
+            for c in hand_over(w_y):
+                handed.append(launch(c))
+
+    hand(wo_y)
+    forward_directions(dq_z, dq_y)
     with jax.named_scope("wait_tp"):
         for c in tiles:
             c.wait_recv()
@@ -415,21 +426,12 @@
     for d in range(1, n):
         k = room(1)
         tiles.append(launch(remote(tile_fs.at[0], tile_fs.at[d], {"fs": (f + d) % n}, k, k)))
-    forward_directions(dq_z, dq_y)
-    relay(wq_z)
-    handed = []
-    if mated:
-        for w_y in (wo_y, wq_y):
-            w_y.wait(z)
-            for c in hand_over(w_y):
-                handed.append(launch(c))
+    forward_directions(do_z, do_y)
+    hand(wq_y)
     for k in range(2, nz - 2):
         forward(k, wo_z, wo_y)
-    for k in range(1, nz - 2):
+    for k in range(1, nz - 1):
         forward(k, wq_z, wq_y)
-    forward_far(wq_z, wq_y, False)
-    forward_far(wq_z, wq_y, True)
-
     with jax.named_scope("wait_fs"):
         for c in tiles:
             c.wait_recv()

time: 42.8 us -> 40.7 us (0.951)
  Pallas kernels: 42 us -> 39.9 us
    pallas_call x1, Pallas kernels: 40.4 us -> 38.3 us  [on_device(): pl.pallas_call(exchange, name='moment_exchange', in_specs=[hbm] * 12, out...]
where the time goes in v3:
time: 40.7 us; the launch traced here: 40.6 us
  Pallas kernels  39.9 us (98%)
  between operations  0.69 us (2%)
    pallas_call x1, Pallas kernels, on_device(): pl.pallas_call(exchange, name='moment_exchange', in_specs=[hbm] * 12, out...  38.3 us
    pallas_call x1, Pallas kernels, on_device(): pl.pallas_call(finish, name='finish', in_specs=[vmem] * 13, out_specs=[hb...  1.58 us

profile of v3, /device:TPU:0, one launch (start us, length us, event | category | flops | bytes accessed | tf_op | source)
XLA Modules:
  0.0 40.6 jit_solution(15194839969826391514)
XLA Ops:
  0.6 0.0 copy-start
  0.7 0.0 copy-start.1
  0.7 38.3 %moment_exchange.1 = (bf16[2,4,2,64,128]{4,3,2,1,0:T(8,128)(2,1)S(1)}, bf16[2,4,2,128,128]{4,3,2,1,0:T(8,128)(2,1)S(1)}, bf16[4,2,64,384]{3,2,1,0:T(8,128)(2,1)S...) custom-call(bf16[3072,512]{1,0:T(8,128)(2,1)} %refs_0_.1, ...), custom_call_target="tpu_custom_call" | custom-call | tf_op jit(solution)/shard_map/moment_exchange/pallas_call | solution.py:542
  39.0 0.0 copy-done
  39.0 0.0 copy-done.1
  39.0 1.6 %finish.1 = (f32[64,384]{1,0:T(8,128)}, f32[128,512]{1,0:T(8,128)}, f32[64,384]{1,0:T(8,128)}, f32[128,512]{1,0:T(8,128)}, bf16[512,384]{1,0:T(8,128)(2,1)}, /*i...) custom-call(bf16[2,4,2,64,128]{4,3,2,1,0:T(8,128)(2,1)S(1)} %get-tup, ...), custom_call_target="tpu_custom_call" | custom-call | tf_op jit(solution)/shard_map/finish/pallas_call | solution.py:607
Async XLA Ops:
  0.6 38.3 %copy-start = (f32[128,512]{1,0:T(8,128)S(1)}, f32[128,512]{1,0:T(8,128)}, u32[]{:S(2)}) copy-start(f32[128,512]{1,0:T(8,128)} %refs_8_.3) | copy-start | bytes 786436
  0.7 38.3 %copy-start.1 = (f32[64,384]{1,0:T(8,128)S(1)}, f32[64,384]{1,0:T(8,128)}, u32[]{:S(2)}) copy-start(f32[64,384]{1,0:T(8,128)} %refs_7_.3) | copy-start | bytes 294916

commit v4 on v3

--- a/solution.py
+++ b/solution.py
@@ -21,7 +21,7 @@
 
 def semaphores_of(nz, ny, nt):
     z_kinds, y_kinds = 2 + 2 + 2 + 2, 2 + 2 + 2
-    return z_kinds * nz + y_kinds * nz * (ny - 1) + 6 * (ny - 1) + 2 * ny + nt + nz * ny + 4
+    return z_kinds * nz + y_kinds * nz * (ny - 1) + 6 * (ny - 1) + 2 * ny + nt + nz * ny + 4 + ny * nt
 
 
 def over_rows(left, right):
@@ -47,6 +47,9 @@
     half = pl.ds(pl.multiple_of(core * half_cols, half_cols), half_cols)
     twin = t + 1 - 2 * (t % 2)
     step = latent_hbm.shape[0] // CHUNKS
+    shares = nt // 2 if fo_hbm.shape[0] % (16 * (nt // 2)) == 0 else 1
+    share_rows = fo_hbm.shape[0] // shares
+    share = pl.ds(pl.multiple_of((t // 2) % shares * share_rows, share_rows), share_rows)
 
     barrier = pltpu.get_barrier_semaphore()
     for d in range(1, n):
@@ -57,7 +60,7 @@
     own = [
         pltpu.make_async_copy(src, dst, own_sem.at[i])
         for i, (src, dst) in enumerate((
-            (fo_hbm.at[:, half], fo_all.at[core, z, y]),
+            (fo_hbm.at[share, half], fo_all.at[core, z, y, share]),
             (fq_hbm.at[:, half], fq_all.at[core, z, y]),
             (wo_hbm, wo), (wq_hbm, wq),
             (om_hbm, om), (os_hbm, os_), (qm_hbm, qm), (qs_hbm, qs),
@@ -157,9 +160,9 @@
                 block = self.block(zz, (y + ny - d) % ny)
                 remote(block, block, {"fs": z * ny + (y + d) % ny}, k, k).wait_recv()
 
-    fo_z = Along(lambda zz: fo_all.at[core, zz, y])
+    fo_z = Along(lambda zz: fo_all.at[core, zz, y, share])
     fq_z = Along(lambda zz: fq_all.at[core, zz, y])
-    fo_y = Across(lambda zz, yy: fo_all.at[core, zz, yy])
+    fo_y = Across(lambda zz, yy: fo_all.at[core, zz, yy, share])
     fq_y = Across(lambda zz, yy: fq_all.at[core, zz, yy])
     wo_z = Along(lambda zz: wo_all.at[zz, y])
     wq_z = Along(lambda zz: wq_all.at[zz, y])
@@ -181,16 +184,17 @@
     inside = jnp.logical_and(z > 0, z < nz - 1)
     far = []
 
-    def send_weights(w_z, ks, relayed=False):
-        for k in ks:
-            c = w_z.to(others[k])
-            if relayed and through and k == nz - 2:
-                far.append(c)
-                pl.when(inside)(c.start)
+    def send_weights(w_z):
+        for k, zz in enumerate(others):
+            c = w_z.to(zz)
+            if through and k > 0:
+                free = jnp.logical_or(
+                    jnp.logical_and(zz > 0, zz < nz - 1), jnp.logical_or(zz == z + 1, zz == z - 1)
+                )
+                far.append((free, c))
+                pl.when(free)(c.start)
             else:
                 launch(c)
-
-    outward = list(reversed(range(nz - 1)))
 
     def product(k, pair, sem, out):
         for c in load(k, pair, sem):
@@ -212,6 +216,19 @@
         block = all_.at[core, :, yy]
         k = room(1)
         return launch(remote(block, block, {"tp": twin}, k, k))
+
+    def to_chips(yy):
+        out = []
+        for d in range(1, shares):
+            block = fo_all.at[core, :, yy, share]
+            k = room(1)
+            out.append(launch(remote(block, block, {"tp": (t + 2 * d) % nt}, k, k)))
+        return out
+
+    def arrived(copies):
+        with jax.named_scope("wait_x"):
+            for c in copies:
+                c.wait_recv()
 
     done = 0
 
@@ -230,15 +247,15 @@
             fq_z.wait(zz)
         fq_y.send(zz)
     swaps["q"] = [swap(fq_all, y)]
-    send_weights(wo_z, outward, True)
+    send_weights(wo_z)
+    send_weights(wq_z)
     for k, zz in enumerate(others):
-        if k == 0:
-            more_o(2)
         with jax.named_scope("wait_foz"):
             fo_z.wait(zz)
         fo_y.send(zz)
-    swaps["o"] = [swap(fo_all, y)]
+    near_o = to_chips(y)
     more_o(CHUNKS - 1)
+    across_o = []
 
     rank = 2 * half_cols
     block = rank // n
@@ -258,19 +275,54 @@
         ("q", fq_all, fq_y, grad_q, rounded_q, part_q, yin_q, acc_q, zout_q, zin_q),
         ("o", fo_all, fo_y, grad_o, rounded_o, part_o, yin_o, acc_o, zout_o, zin_o),
     )
+    ahead = []
+
+    def relay(w_z, ks):
+        for k in ks if through else ():
+            mine = []
+            for edge, here in ((0, 1), (nz - 1, nz - 2)):
+                at = room(1)
+                mine.append((here, remote(
+                    w_z.block(others[k]), w_z.block(others[k]), {"fs": edge * ny + y},
+                    at, w_z.at + others[k],
+                )))
+            with jax.named_scope("wait_far"):
+                pl.when(inside)(lambda: w_z.wait(others[k]))
+            for here, c in mine:
+                pl.when(z == here)(c.start)
+            ahead.extend(mine)
+
+    def pass_on(w_z, w_y, k):
+        with jax.named_scope("wait_edge"):
+            if through:
+                pl.when(jnp.logical_not(inside))(lambda: w_z.wait(others[k]))
+            else:
+                w_z.wait(others[k])
+        w_y.send(others[k])
+
     units = []
     for name, all_, fac_y, grad, rounded, part, yin, acc, zout, zin in matrices:
         if name == "o":
             wq_y.send(z)
             more_o(CHUNKS)
+            arrived(across_o)
         rounded[...] = grad[...].astype(BF16)
         along = Along(lambda zz, zout=zout: zout.at[zz], lambda zz, zin=zin: zin.at[zz])
-        with jax.named_scope("wait_fy"):
-            for zz in [z] + others:
-                fac_y.wait(zz)
+        if name == "q":
+            with jax.named_scope("wait_fy"):
+                for zz in [z] + others:
+                    fac_y.wait(zz)
         for d in range(1, ny):
             swaps[name].append(swap(all_, (y + ny - d) % ny))
         for turn, h in enumerate((core, 1 - core)):
+            if turn and name == "q":
+                with jax.named_scope("wait_foy"):
+                    for zz in [z] + others:
+                        fo_y.wait(zz)
+                for d in range(1, ny):
+                    across_o += to_chips((y + ny - d) % ny)
+                arrived(near_o)
+                swaps["o"] = [swap(fo_all, y)]
             if turn:
                 with jax.named_scope("wait_swap"):
                     for c in swaps[name]:
@@ -287,6 +339,10 @@
                 copies.append(launch(remote(
                     yin.at[ny - 1 + d - 1, rows], yin.at[d - 1, rows], {"fs": z * ny + yy}, k, k
                 )))
+            if name == "q" and turn == 1:
+                relay(wo_z, range(1, min(2, nz - 1)))
+            if name == "o" and turn == 0:
+                relay(wo_z, range(2, nz - 1))
             units.append((h, part, yin, acc, zout, along, copies))
 
     def forward(k, w_z, w_y):
@@ -297,42 +353,6 @@
     if nz > 1 and not mated:
         forward(0, wo_z, wo_y)
         forward(0, wq_z, wq_y)
-
-    ahead = []
-
-    def relay(w_z):
-        if not through:
-            return
-        mine = []
-        for edge, here in ((0, nz - 2), (nz - 1, 1)):
-            k = room(1)
-            mine.append((here, remote(
-                w_z.block(edge), w_z.block(edge), {"fs": (nz - 1 - edge) * ny + y},
-                k, w_z.at + edge,
-            )))
-
-        @pl.when(inside)
-        def _():
-            with jax.named_scope("wait_far"):
-                w_z.wait(others[nz - 2])
-        for here, c in mine:
-            pl.when(z == here)(c.start)
-        ahead.extend(mine)
-
-    def forward_far(w_z, w_y, at_edge):
-        if not through:
-            return
-        if at_edge:
-            @pl.when(jnp.logical_not(inside))
-            def _():
-                with jax.named_scope("wait_wz_last"):
-                    w_z.wait(others[nz - 2])
-        cs = w_y.copies(others[nz - 2])
-        for c in cs:
-            pl.when(jnp.logical_not(inside) if at_edge else inside)(c.start)
-        fars.append((at_edge, cs))
-
-    fars = []
 
     def hand_over(w_y):
         mate = z + 1 - 2 * (z % 2)
@@ -348,10 +368,10 @@
 
     low_sent = []
     for turn, (h, part, yin, acc, zout, along, copies) in enumerate(units):
-        if turn == 2:
-            relay(wo_z)
-        if turn == 3 and nz > 3:
-            forward(1, wo_z, wo_y)
+        if turn == 3:
+            relay(wq_z, range(1, nz - 1))
+        if turn == 3 and nz > 2:
+            pass_on(wo_z, wo_y, 1)
         for i in range(per_half):
             acc[h * per_half + i] = part[h * per_half + i, y]
         for d, c in enumerate(copies):
@@ -370,7 +390,8 @@
         (matrices[0], units[0][5], qm, qs, qm_new, qs_new, dq_all, dq_z, dq_y),
         (matrices[1], units[2][5], om, os_, om_new, os_new, do_all, do_z, do_y),
     )
-    forward_far(wo_z, wo_y, False)
+    for k in range(2, nz - 1):
+        pass_on(wo_z, wo_y, k)
     for c in own[4:]:
         c.wait()
     squares = []
@@ -392,7 +413,7 @@
         d_y.send(z)
         squares.append(jnp.sum(direction * direction))
         if len(squares) == 1:
-            forward_far(wo_z, wo_y, True)
+            pass
     lanes = lax.broadcasted_iota(jnp.int32, tile_tp.shape[1:], 1)
     tile_tp[0] = jnp.where(lanes < tile_tp.shape[2] // 2, squares[0], squares[1])
 
@@ -400,7 +421,6 @@
     for d in range(1, nt):
         k = room(1)
         tiles.append(launch(remote(tile_tp.at[0], tile_tp.at[d], {"tp": (t + d) % nt}, k, k)))
-    send_weights(wq_z, outward)
 
     def forward_directions(d_z, d_y):
         for zz in others:
@@ -416,8 +436,9 @@
             for c in hand_over(w_y):
                 handed.append(launch(c))
 
-    hand(wo_y)
     forward_directions(dq_z, dq_y)
+    for k in range(1, nz - 1):
+        pass_on(wq_z, wq_y, k)
     with jax.named_scope("wait_tp"):
         for c in tiles:
             c.wait_recv()
@@ -427,11 +448,8 @@
         k = room(1)
         tiles.append(launch(remote(tile_fs.at[0], tile_fs.at[d], {"fs": (f + d) % n}, k, k)))
     forward_directions(do_z, do_y)
+    hand(wo_y)
     hand(wq_y)
-    for k in range(2, nz - 2):
-        forward(k, wo_z, wo_y)
-    for k in range(1, nz - 1):
-        forward(k, wq_z, wq_y)
     with jax.named_scope("wait_fs"):
         for c in tiles:
             c.wait_recv()
@@ -454,13 +472,10 @@
             c.wait_send()
     for zz, c in low_sent:
         pl.when(zz != z)(c.wait_send)
-    for c in far:
-        pl.when(inside)(c.wait_send)
+    for free, c in far:
+        pl.when(free)(c.wait_send)
     for here, c in ahead:
         pl.when(z == here)(c.wait_send)
-    for at_edge, cs in fars:
-        for c in cs:
-            pl.when(jnp.logical_not(inside) if at_edge else inside)(c.wait_send)
 
 
 def finish_kernel(

time: 40.7 us -> 39.7 us (0.975)
  Pallas kernels: 39.9 us -> 38.9 us
    pallas_call x1, Pallas kernels: 38.3 us -> 37.3 us  [on_device(): pl.pallas_call(exchange, name='moment_exchange', in_specs=[hbm] * 12, out...]
where the time goes in v4:
time: 39.7 us; the launch traced here: 39.6 us
  Pallas kernels  38.9 us (98%)
  between operations  0.69 us (2%)
    pallas_call x1, Pallas kernels, on_device(): pl.pallas_call(exchange, name='moment_exchange', in_specs=[hbm] * 12, out...  37.3 us
    pallas_call x1, Pallas kernels, on_device(): pl.pallas_call(finish, name='finish', in_specs=[vmem] * 13, out_specs=[hb...  1.58 us

profile of v4, /device:TPU:0, one launch (start us, length us, event | category | flops | bytes accessed | tf_op | source)
XLA Modules:
  0.0 39.6 jit_solution(10988761952247075418)
XLA Ops:
  0.6 0.0 copy-start
  0.7 0.0 copy-start.1
  0.7 37.3 %moment_exchange.1 = (bf16[2,4,2,64,128]{4,3,2,1,0:T(8,128)(2,1)S(1)}, bf16[2,4,2,128,128]{4,3,2,1,0:T(8,128)(2,1)S(1)}, bf16[4,2,64,384]{3,2,1,0:T(8,128)(2,1)S...) custom-call(bf16[3072,512]{1,0:T(8,128)(2,1)} %refs_0_.1, ...), custom_call_target="tpu_custom_call" | custom-call | tf_op jit(solution)/shard_map/moment_exchange/pallas_call | solution.py:557
  37.9 0.0 copy-done
  38.0 0.0 copy-done.1
  38.0 1.6 %finish.1 = (f32[64,384]{1,0:T(8,128)}, f32[128,512]{1,0:T(8,128)}, f32[64,384]{1,0:T(8,128)}, f32[128,512]{1,0:T(8,128)}, bf16[512,384]{1,0:T(8,128)(2,1)}, /*i...) custom-call(bf16[2,4,2,64,128]{4,3,2,1,0:T(8,128)(2,1)S(1)} %get-tup, ...), custom_call_target="tpu_custom_call" | custom-call | tf_op jit(solution)/shard_map/finish/pallas_call | solution.py:622
Async XLA Ops:
  0.6 37.3 %copy-start = (f32[128,512]{1,0:T(8,128)S(1)}, f32[128,512]{1,0:T(8,128)}, u32[]{:S(2)}) copy-start(f32[128,512]{1,0:T(8,128)} %refs_8_.3) | copy-start | bytes 786436
  0.7 37.3 %copy-start.1 = (f32[64,384]{1,0:T(8,128)S(1)}, f32[64,384]{1,0:T(8,128)}, u32[]{:S(2)}) copy-start(f32[64,384]{1,0:T(8,128)} %refs_7_.3) | copy-start | bytes 294916

commit v5 on v4

--- a/solution.py
+++ b/solution.py
@@ -390,8 +390,6 @@
         (matrices[0], units[0][5], qm, qs, qm_new, qs_new, dq_all, dq_z, dq_y),
         (matrices[1], units[2][5], om, os_, om_new, os_new, do_all, do_z, do_y),
     )
-    for k in range(2, nz - 1):
-        pass_on(wo_z, wo_y, k)
     for c in own[4:]:
         c.wait()
     squares = []
@@ -413,7 +411,8 @@
         d_y.send(z)
         squares.append(jnp.sum(direction * direction))
         if len(squares) == 1:
-            pass
+            for k in range(2, nz - 1):
+                pass_on(wo_z, wo_y, k)
     lanes = lax.broadcasted_iota(jnp.int32, tile_tp.shape[1:], 1)
     tile_tp[0] = jnp.where(lanes < tile_tp.shape[2] // 2, squares[0], squares[1])
 
@@ -422,8 +421,8 @@
         k = room(1)
         tiles.append(launch(remote(tile_tp.at[0], tile_tp.at[d], {"tp": (t + d) % nt}, k, k)))
 
-    def forward_directions(d_z, d_y):
-        for zz in others:
+    def forward_directions(d_z, d_y, ks):
+        for zz in [others[k] for k in ks]:
             with jax.named_scope("wait_dz"):
                 d_z.wait(zz)
             d_y.send(zz)
@@ -436,9 +435,10 @@
             for c in hand_over(w_y):
                 handed.append(launch(c))
 
-    forward_directions(dq_z, dq_y)
+    forward_directions(dq_z, dq_y, range(nz - 1))
     for k in range(1, nz - 1):
         pass_on(wq_z, wq_y, k)
+    forward_directions(do_z, do_y, range(min(1, nz - 1)))
     with jax.named_scope("wait_tp"):
         for c in tiles:
             c.wait_recv()
@@ -447,9 +447,9 @@
     for d in range(1, n):
         k = room(1)
         tiles.append(launch(remote(tile_fs.at[0], tile_fs.at[d], {"fs": (f + d) % n}, k, k)))
-    forward_directions(do_z, do_y)
     hand(wo_y)
     hand(wq_y)
+    forward_directions(do_z, do_y, range(1, nz - 1))
     with jax.named_scope("wait_fs"):
         for c in tiles:
             c.wait_recv()

time: 39.7 us -> 39.2 us (0.987)
  Pallas kernels: 38.9 us -> 38.4 us
    pallas_call x1, Pallas kernels: 37.3 us -> 36.8 us  [on_device(): pl.pallas_call(exchange, name='moment_exchange', in_specs=[hbm] * 12, out...]
where the time goes in v5:
time: 39.2 us; the launch traced here: 39.1 us
  Pallas kernels  38.4 us (98%)
  between operations  0.69 us (2%)
    pallas_call x1, Pallas kernels, on_device(): pl.pallas_call(exchange, name='moment_exchange', in_specs=[hbm] * 12, out...  36.8 us
    pallas_call x1, Pallas kernels, on_device(): pl.pallas_call(finish, name='finish', in_specs=[vmem] * 13, out_specs=[hb...  1.58 us

profile of v5, /device:TPU:0, one launch (start us, length us, event | category | flops | bytes accessed | tf_op | source)
XLA Modules:
  0.0 39.1 jit_solution(5074576015333725417)
XLA Ops:
  0.6 0.0 copy-start
  0.7 0.0 copy-start.1
  0.7 36.8 %moment_exchange.1 = (bf16[2,4,2,64,128]{4,3,2,1,0:T(8,128)(2,1)S(1)}, bf16[2,4,2,128,128]{4,3,2,1,0:T(8,128)(2,1)S(1)}, bf16[4,2,64,384]{3,2,1,0:T(8,128)(2,1)S...) custom-call(bf16[3072,512]{1,0:T(8,128)(2,1)} %refs_0_.1, ...), custom_call_target="tpu_custom_call" | custom-call | tf_op jit(solution)/shard_map/moment_exchange/pallas_call | solution.py:557
  37.5 0.0 copy-done
  37.5 0.0 copy-done.1
  37.5 1.6 %finish.1 = (f32[64,384]{1,0:T(8,128)}, f32[128,512]{1,0:T(8,128)}, f32[64,384]{1,0:T(8,128)}, f32[128,512]{1,0:T(8,128)}, bf16[512,384]{1,0:T(8,128)(2,1)}, /*i...) custom-call(bf16[2,4,2,64,128]{4,3,2,1,0:T(8,128)(2,1)S(1)} %get-tup, ...), custom_call_target="tpu_custom_call" | custom-call | tf_op jit(solution)/shard_map/finish/pallas_call | solution.py:622
Async XLA Ops:
  0.6 36.8 %copy-start = (f32[128,512]{1,0:T(8,128)S(1)}, f32[128,512]{1,0:T(8,128)}, u32[]{:S(2)}) copy-start(f32[128,512]{1,0:T(8,128)} %refs_8_.3) | copy-start | bytes 786436
  0.7 36.8 %copy-start.1 = (f32[64,384]{1,0:T(8,128)S(1)}, f32[64,384]{1,0:T(8,128)}, u32[]{:S(2)}) copy-start(f32[64,384]{1,0:T(8,128)} %refs_7_.3) | copy-start | bytes 294916
